TPU v7x, 32 devices: a whole 2x2x4 slice. The times are simulated.
32 devices in a mesh: ep: 16 (over z, y, x), tp: 2 (over core).
Axes of the slice: x: 2, y: 2, z: 4, core: 2. Of those that a mesh axis runs over, the one named last changes fastest.
Arguments:
- tokens: bfloat16 [512, 2048], P('ep', 'tp')
- norm1_gain: float32 [2048], P('tp'), may hold values from 0.1 to 1.9
- w_query: bfloat16 [2048, 1024], P('tp'), may hold values from -0.125 to 0.125
- w_key: bfloat16 [2048, 128], P('tp'), may hold values from -0.125 to 0.125
- w_value: bfloat16 [2048, 128], P('tp'), may hold values from -0.125 to 0.125
- head_bias: float32 [16], P('tp'), may hold values from -7 to -1.5
- key_cache: bfloat16 [512, 1024, 128], P('ep', None, 'tp'), may hold values from -6 to 6
- value_cache: bfloat16 [512, 1024, 128], P('ep', None, 'tp'), may hold values from -6 to 6
- seq_lengths: int32 [512], P('ep'), may hold values from 1 to 1024, as said below
- w_out: bfloat16 [1024, 2048], P('tp'), may hold values from -0.375 to 0.375
- norm2_gain: float32 [2048], P('tp'), may hold values from 0.5 to 8
- route_ids: int32 [512, 4], P('ep'), may hold values from 0 to 15, all different within a row; in each aligned block of 32 rows (0 to 31, 32 to 63, ...) at most 16 rows name the same one
- route_logits: float32 [512, 4], P('ep'), may hold values from -6 to 6
- expert_gate: bfloat16 [16, 2048, 2048], P('ep', None, 'tp'), may hold values from -0.125 to 0.125
- expert_up: bfloat16 [16, 2048, 2048], P('ep', None, 'tp'), may hold values from -0.125 to 0.125
- expert_down: bfloat16 [16, 2048, 2048], P('ep', 'tp'), may hold values from -0.125 to 0.125
Outputs:
- mixed_out: bfloat16 [512, 2048], P('ep', 'tp')
- new_key: bfloat16 [512, 128], P('ep', 'tp')
- new_value: bfloat16 [512, 128], P('ep', 'tp')
Inputs may be any that keep to these rules, and one draw needn't show every extreme that they name: A sequence attends to its first seq_lengths cache positions; in every draw some sequence has exactly 1024. `route_ids`: each row names 4 different experts. Among the rows of one device no expert is named more than 16 times, and in every draw some expert is named exactly 16 times by some device's rows.
All inputs are finite; a program needn't handle non-finite values.
Results may differ from a plain program's by a relative error of at most 0.028.
Values may be sent and summed in bfloat16 or wider, within the bound.
A program may use at most 128 MiB of HBM per device.

v0:
```python
import functools

import jax
import jax.numpy as jnp
from jax import lax
from jax.experimental import pallas as pl
from jax.experimental.pallas import tpu as pltpu
from jax.sharding import PartitionSpec as P

HEAD = 64
LN_EPS = 1e-05
SWIGLU_ALPHA = 1.702
SWIGLU_LIMIT = 7.0
MESH = pl.DeviceIdType.MESH
F32 = jnp.float32
BF16 = jnp.bfloat16
DEAD = -1e30
POS_BLOCK = 256
COL_BLOCK = 256


def dot(a, b):
    return jnp.dot(a, b, preferred_element_type=F32)


def kernel(
    n,
    cap,
    tok_hbm,
    g1_hbm,
    wq_hbm,
    wk_hbm,
    wv_hbm,
    bias_ref,
    kc_hbm,
    vc_hbm,
    lens_ref,
    wo_hbm,
    g2_hbm,
    ids_hbm,
    logits_hbm,
    gate_hbm,
    up_hbm,
    down_hbm,
    out_ref,
    nk_ref,
    nv_ref,
    x_own,
    x_peer,
    g1,
    wq,
    wk,
    wv,
    kc,
    vc,
    wo,
    g2,
    ids,
    logits,
    gate,
    up,
    down,
    proj_send,
    proj_recv,
    q_rows,
    z_ref,
    att_ref,
    part_send,
    part_recv,
    res_ref,
    tables_send,
    tables_recv,
    rows_ref,
    rows_recv,
    disp,
    recv_own,
    recv_peer,
    gate_acc,
    up_acc,
    act_ref,
    down_send,
    down_recv,
    down_own,
    back_send,
    back_recv,
    sum_send,
    sum_recv,
    load_sem,
    one_send,
    one_recv,
    table_send_sem,
    table_recv_sem,
    rows_send_sem,
    rows_recv_sem,
    sum_send_sem,
    sum_recv_sem,
    disp_send_sem,
    disp_recv_sem,
    fwd_send_sem,
    fwd_recv_sem,
    down_send_sem,
    down_recv_sem,
    back_send_sem,
    back_recv_sem,
    local_sem,
):
    ep = lax.axis_index("ep")
    tp = lax.axis_index("tp")
    other = 1 - tp
    seqs, half = x_own.shape
    width = 2 * half
    slots = n * cap

    loads = []
    pairs = (
        (tok_hbm, x_own),
        (g1_hbm, g1),
        (wq_hbm, wq),
        (wk_hbm, wk),
        (wv_hbm, wv),
        (kc_hbm, kc),
        (vc_hbm, vc),
        (wo_hbm, wo),
        (g2_hbm, g2),
        (ids_hbm, ids),
        (logits_hbm, logits),
        (gate_hbm, gate),
        (up_hbm, up),
        (down_hbm, down),
    )
    for i, (src, dst) in enumerate(pairs):
        copy = pltpu.make_async_copy(src, dst, load_sem.at[i])
        loads.append(copy)
    for i in (0, 2, 3, 4, 1, 9, 10, 8):
        loads[i].start()

    def peer_copy(src, dst, i):
        return pltpu.make_async_remote_copy(
            src_ref=src,
            dst_ref=dst,
            send_sem=one_send.at[i],
            recv_sem=one_recv.at[i],
            device_id=(ep, other),
            device_id_type=MESH,
        )

    barrier = pltpu.get_barrier_semaphore()
    pl.semaphore_signal(barrier, inc=1, device_id=(ep, other), device_id_type=MESH)

    planes = tables_send.shape[0]
    plane = n // planes
    level = ep // plane
    spot = ep % plane

    def column(i):
        return lax.rem(level + i, planes) * plane + spot

    def beside(i):
        return level * plane + lax.rem(spot + i, plane)

    def greet_column(i, carry):
        pl.semaphore_signal(barrier, inc=1, device_id=(column(i), tp), device_id_type=MESH)
        return carry

    def greet_beside(i, carry):
        pl.semaphore_signal(barrier, inc=1, device_id=(beside(i), tp), device_id_type=MESH)
        return carry

    lax.fori_loop(1, planes, greet_column, 0)
    lax.fori_loop(1, plane, greet_beside, 0)
    pl.semaphore_wait(barrier, planes + plane - 1)

    loads[0].wait()
    tok_copy = peer_copy(x_own, x_peer, 0)
    tok_copy.start()
    loads[1].wait()
    for i in (2, 3, 4):
        loads[i].wait()
    for i in (5, 6, 7):
        loads[i].start()
    mine = x_own[...].astype(F32)
    tok_copy.wait()
    theirs = x_peer[...].astype(F32)

    def stats(a, b):
        total = jnp.sum(a, axis=1, keepdims=True) + jnp.sum(b, axis=1, keepdims=True)
        square = jnp.sum(a * a, axis=1, keepdims=True) + jnp.sum(b * b, axis=1, keepdims=True)
        mean = total / width
        return mean, lax.rsqrt(square / width - mean * mean + LN_EPS)

    mean, scale = stats(mine, theirs)
    normed = ((mine - mean) * scale * g1[...]).astype(BF16)
    pq = dot(normed, wq[...])
    pk = dot(normed, wk[...])
    pv = dot(normed, wv[...])
    qc = pq.shape[1] // 2
    kcols = pk.shape[1] // 2
    first = tp == 0
    proj_send[:, :qc] = jnp.where(first, pq[:, qc:], pq[:, :qc])
    proj_send[:, qc : qc + kcols] = jnp.where(first, pk[:, kcols:], pk[:, :kcols])
    proj_send[:, qc + kcols :] = jnp.where(first, pv[:, kcols:], pv[:, :kcols])
    proj_copy = peer_copy(proj_send, proj_recv, 1)
    proj_copy.start()

    for i in (11, 12, 13):
        loads[i].start()
    loads[9].wait()
    loads[10].wait()
    top = ids.shape[0]
    slot_row = lax.broadcasted_iota(jnp.int32, (slots, seqs), 0)
    slot_expert = slot_row // cap
    slot_rank = slot_row - slot_expert * cap
    id_rows = ids[...]
    raw = jnp.exp(logits[...])
    probs = raw / jnp.sum(raw, axis=0, keepdims=True)
    hot = jnp.zeros((slots, seqs), F32)
    prob_hot = jnp.zeros((slots, seqs), F32)
    for k in range(top):
        match = id_rows[k : k + 1, :] == slot_expert
        hot = hot + jnp.where(match, 1.0, 0.0)
        prob_hot = prob_hot + jnp.where(match, probs[k : k + 1, :], 0.0)
    earlier = (
        lax.broadcasted_iota(jnp.int32, (seqs, seqs), 0)
        < lax.broadcasted_iota(jnp.int32, (seqs, seqs), 1)
    )
    rank = dot(hot.astype(BF16), jnp.where(earlier, 1.0, 0.0).astype(BF16))
    chosen = (hot > 0.5) & (jnp.abs(rank - slot_rank.astype(F32)) < 0.5)
    placing = jnp.where(chosen, 1.0, 0.0).astype(BF16)
    weight = jnp.where(chosen, prob_hot, 0.0)
    weight_hi = weight.astype(BF16)
    weight_lo = (weight - weight_hi.astype(F32)).astype(BF16)
    group = plane * cap
    for q in range(planes):
        at = slice(q * group, (q + 1) * group)
        tables_send[q, 0] = placing[at]
        tables_send[q, 1] = weight_hi[at]
        tables_send[q, 2] = weight_lo[at]

    groups = qc // HEAD
    bias = jnp.zeros((groups, 1), F32)
    head_row = lax.broadcasted_iota(jnp.int32, (groups, 1), 0)
    for h in range(groups):
        bias = bias + jnp.where(head_row == h, bias_ref[h], 0.0)

    own_q = jnp.where(first, pq[:, :qc], pq[:, qc:])
    own_k = jnp.where(first, pk[:, :kcols], pk[:, kcols:])
    own_v = jnp.where(first, pv[:, :kcols], pv[:, kcols:])
    proj_copy.wait()
    query = (own_q + proj_recv[:, :qc]).astype(BF16).astype(F32)
    nk_ref[...] = (own_k + proj_recv[:, qc : qc + kcols]).astype(BF16)
    nv_ref[...] = (own_v + proj_recv[:, qc + kcols :]).astype(BF16)
    for h in range(groups):
        q_rows[:, h, :] = query[:, h * HEAD : (h + 1) * HEAD]

    def to_column(src, dst, sends, recvs, i):
        to = lax.rem(level + i, planes)
        return pltpu.make_async_remote_copy(
            src_ref=src.at[to],
            dst_ref=dst.at[level],
            send_sem=sends.at[i],
            recv_sem=recvs.at[i],
            device_id=(column(i), tp),
            device_id_type=MESH,
        )

    def from_column(src, dst, sends, recvs, i):
        source = lax.rem(level + planes - i, planes)
        return pltpu.make_async_remote_copy(
            src_ref=src.at[source],
            dst_ref=dst.at[source],
            send_sem=sends.at[i],
            recv_sem=recvs.at[i],
            device_id=(source * plane + spot, tp),
            device_id_type=MESH,
        )

    table_args = (tables_send, tables_recv, table_send_sem, table_recv_sem)
    for i in range(1, planes):
        to_column(*table_args, i).start()
    tables_recv[level] = tables_send[level]

    positions = kc.shape[2]
    loads[5].wait()
    place = lax.broadcasted_iota(jnp.int32, (groups, positions), 1)

    def score_step(i, carry):
        for j in range(4):
            b = i * 4 + j
            s = dot(q_rows[b].astype(BF16), kc[b]) * HEAD ** (-0.5) + bias
            z_ref[pl.ds(pl.multiple_of(b * groups, groups), groups), :] = jnp.where(
                place < lens_ref[b], s, DEAD
            )
        return carry

    lax.fori_loop(0, seqs // 4, score_step, 0)

    after = (
        lax.broadcasted_iota(jnp.int32, (POS_BLOCK, POS_BLOCK), 0)
        > lax.broadcasted_iota(jnp.int32, (POS_BLOCK, POS_BLOCK), 1)
    )
    after = jnp.where(after, 1.0, 0.0).astype(BF16)
    row_block = 64

    def break_step(i, carry):
        rows = pl.ds(pl.multiple_of(i * row_block, row_block), row_block)
        beyond = jnp.zeros((row_block, 1), F32)
        for c in reversed(range(positions // POS_BLOCK)):
            cols = slice(c * POS_BLOCK, (c + 1) * POS_BLOCK)
            z = z_ref[rows, cols]
            tail = jnp.log1p(jnp.exp(-jnp.abs(z)))
            spent = jnp.maximum(z, 0.0) + tail
            hi = spent.astype(BF16)
            lo = (spent - hi.astype(F32)).astype(BF16)
            sums = dot(jnp.concatenate([hi, lo], axis=0), after)
            inside = sums[:row_block] + sums[row_block:]
            z_ref[rows, cols] = jnp.exp(jnp.minimum(z, 0.0) - tail - (inside + beyond))
            beyond = beyond + inside[:, :1] + spent[:, :1]
        return carry

    lax.fori_loop(0, seqs * groups // row_block, break_step, 0)

    loads[6].wait()

    def read_step(i, carry):
        rows = pl.ds(pl.multiple_of(i * 4 * groups, 4 * groups), 4 * groups)
        weights = z_ref[rows, :].astype(BF16)
        values = vc[pl.ds(i * 4, 4)].reshape(4 * HEAD, positions)
        mixed = lax.dot_general(
            weights, values, (((1,), (1,)), ((), ())), preferred_element_type=F32
        )
        for j in range(4):
            att_ref[i * 4 + j] = mixed[
                j * groups : (j + 1) * groups, j * HEAD : (j + 1) * HEAD
            ]
        return carry

    lax.fori_loop(0, seqs // 4, read_step, 0)
    attended = jnp.concatenate([att_ref[:, h, :] for h in range(groups)], axis=1).astype(BF16)

    loads[7].wait()
    part = dot(attended, wo[...]).astype(BF16)
    part_send[0] = part[:, :half]
    part_send[1] = part[:, half:]
    part_copy = peer_copy(part_send, part_recv, 2)
    part_copy.start()
    loads[8].wait()
    part_copy.wait()
    mine = x_own[...].astype(F32)
    theirs = x_peer[...].astype(F32)
    res_own = (mine + (part_send[tp].astype(F32) + part_recv[tp].astype(F32))).astype(BF16)
    res_other = (
        theirs + (part_send[other].astype(F32) + part_recv[other].astype(F32))
    ).astype(BF16)
    res_ref[...] = res_own
    mine = res_own.astype(F32)
    mean, scale = stats(mine, res_other.astype(F32))
    normed_two = ((mine - mean) * scale * g2[...]).astype(BF16)
    rows_ref[...] = normed_two

    def rows_copy(i):
        return pltpu.make_async_remote_copy(
            src_ref=rows_ref,
            dst_ref=rows_recv.at[level],
            send_sem=rows_send_sem.at[i],
            recv_sem=rows_recv_sem.at[i],
            device_id=(column(i), tp),
            device_id_type=MESH,
        )

    def rows_arrival(i):
        source = lax.rem(level + planes - i, planes)
        return pltpu.make_async_remote_copy(
            src_ref=rows_ref,
            dst_ref=rows_recv.at[source],
            send_sem=rows_send_sem.at[i],
            recv_sem=rows_recv_sem.at[i],
            device_id=(source * plane + spot, tp),
            device_id_type=MESH,
        )

    def beside_copy(src, dst, sends, recvs, i, j):
        source = lax.rem(level + planes - i, planes)
        to = lax.rem(spot + j, plane)
        return pltpu.make_async_remote_copy(
            src_ref=src.at[source, to],
            dst_ref=dst.at[source, spot],
            send_sem=sends.at[i, j],
            recv_sem=recvs.at[i, j],
            device_id=(level * plane + to, tp),
            device_id_type=MESH,
        )

    def beside_arrival(src, dst, sends, recvs, i, j):
        source = lax.rem(level + planes - i, planes)
        giver = lax.rem(spot + plane - j, plane)
        return pltpu.make_async_remote_copy(
            src_ref=src.at[source, giver],
            dst_ref=dst.at[source, giver],
            send_sem=sends.at[i, j],
            recv_sem=recvs.at[i, j],
            device_id=(level * plane + giver, tp),
            device_id_type=MESH,
        )

    def fwd_copy(i, j):
        source = lax.rem(level + planes - i, planes)
        giver = lax.rem(spot + plane - j, plane)
        return pltpu.make_async_remote_copy(
            src_ref=recv_own.at[source, giver],
            dst_ref=recv_peer.at[source, giver],
            send_sem=fwd_send_sem.at[i, j],
            recv_sem=fwd_recv_sem.at[i, j],
            device_id=(ep, other),
            device_id_type=MESH,
        )

    disp_args = (disp, recv_own, disp_send_sem, disp_recv_sem)
    for i in range(1, planes):
        rows_copy(i).start()
    for i in range(1, planes):
        from_column(*table_args, i).wait_recv()
    keeps = []

    def place_rows(i, rows):
        source = lax.rem(level + planes - i, planes)
        placed = dot(tables_recv[source, 0], rows).astype(BF16)
        disp[source] = placed.reshape(plane, cap, half)
        for j in range(1, plane):
            beside_copy(*disp_args, i, j).start()
        keep = pltpu.make_async_copy(
            disp.at[source, spot], recv_own.at[source, spot], local_sem.at[i]
        )
        keep.start()
        keeps.append(keep)

    place_rows(0, normed_two)
    for i in range(1, planes):
        rows_arrival(i).wait_recv()
        place_rows(i, rows_recv[lax.rem(level + planes - i, planes)])
    for i in range(planes):
        keeps[i].wait()
        fwd_copy(i, 0).start()
        for j in range(1, plane):
            beside_arrival(*disp_args, i, j).wait_recv()
            fwd_copy(i, j).start()

    loads[11].wait()
    loads[12].wait()
    rows_block = min(slots, 256)
    row_blocks = slots // rows_block
    per_block = rows_block // group
    hidden = gate.shape[1]

    def first_half(i, carry):
        cols = pl.ds(pl.multiple_of(i * COL_BLOCK, COL_BLOCK), COL_BLOCK)
        depth = pl.ds(pl.multiple_of(tp * half, half), half)
        for r in range(row_blocks):
            rows = recv_own[r * per_block : (r + 1) * per_block].reshape(rows_block, half)
            at = slice(r * rows_block, (r + 1) * rows_block)
            gate_acc[at, cols] = dot(rows, gate[depth, cols])
            up_acc[at, cols] = dot(rows, up[depth, cols])
        return carry

    lax.fori_loop(0, hidden // COL_BLOCK, first_half, 0)

    for i in range(planes):
        for j in range(plane):
            fwd_copy(i, j).wait()

    def second_half(i, carry):
        cols = pl.ds(pl.multiple_of(i * COL_BLOCK, COL_BLOCK), COL_BLOCK)
        depth = pl.ds(pl.multiple_of(other * half, half), half)
        for r in range(row_blocks):
            rows = recv_peer[r * per_block : (r + 1) * per_block].reshape(rows_block, half)
            at = slice(r * rows_block, (r + 1) * rows_block)
            g = gate_acc[at, cols] + dot(rows, gate[depth, cols])
            u = up_acc[at, cols] + dot(rows, up[depth, cols])
            c = jnp.minimum(g, SWIGLU_LIMIT)
            linear = jnp.clip(u, -SWIGLU_LIMIT, SWIGLU_LIMIT)
            act_ref[at, cols] = (
                c * jax.nn.sigmoid(SWIGLU_ALPHA * c) * (linear + 1.0)
            ).astype(BF16)
        return carry

    lax.fori_loop(0, hidden // COL_BLOCK, second_half, 0)

    loads[13].wait()
    tiles = half // COL_BLOCK

    def down_copy(i):
        return pltpu.make_async_remote_copy(
            src_ref=down_send.at[i],
            dst_ref=down_recv.at[i],
            send_sem=down_send_sem.at[i],
            recv_sem=down_recv_sem.at[i],
            device_id=(ep, other),
            device_id_type=MESH,
        )

    def down_tile(ref, side, i):
        cols = pl.ds(pl.multiple_of(side * half + i * COL_BLOCK, COL_BLOCK), COL_BLOCK)
        for r in range(row_blocks):
            at = slice(r * rows_block, (r + 1) * rows_block)
            ref[i, at, :] = dot(act_ref[at, :], down[:, cols]).astype(BF16)

    def down_other(i, carry):
        down_tile(down_send, other, i)
        down_copy(i).start()
        return carry

    lax.fori_loop(0, tiles, down_other, 0)

    def down_mine(i, carry):
        down_tile(down_own, tp, i)
        return carry

    lax.fori_loop(0, tiles, down_mine, 0)
    for i in range(tiles):
        down_copy(i).wait()
        total = (down_own[i].astype(F32) + down_recv[i].astype(F32)).astype(BF16)
        back_send[:, :, :, i * COL_BLOCK : (i + 1) * COL_BLOCK] = total.reshape(
            planes, plane, cap, COL_BLOCK
        )

    back_args = (back_send, back_recv, back_send_sem, back_recv_sem)
    order = tuple(range(1, planes)) + (0,)
    back_keeps = {}
    for i in order:
        for j in range(1, plane):
            beside_copy(*back_args, i, j).start()
        source = lax.rem(level + planes - i, planes)
        back_keeps[i] = pltpu.make_async_copy(
            back_send.at[source, spot], back_recv.at[source, spot], local_sem.at[planes + i]
        )
        back_keeps[i].start()

    def sum_copy(i):
        source = lax.rem(level + planes - i, planes)
        return pltpu.make_async_remote_copy(
            src_ref=sum_send.at[source],
            dst_ref=sum_recv.at[level],
            send_sem=sum_send_sem.at[i],
            recv_sem=sum_recv_sem.at[i],
            device_id=(source * plane + spot, tp),
            device_id_type=MESH,
        )

    def sum_arrival(i):
        giver = lax.rem(level + i, planes)
        return pltpu.make_async_remote_copy(
            src_ref=sum_send.at[giver],
            dst_ref=sum_recv.at[giver],
            send_sem=sum_send_sem.at[i],
            recv_sem=sum_recv_sem.at[i],
            device_id=(giver * plane + spot, tp),
            device_id_type=MESH,
        )

    over_slots = (((0,), (0,)), ((), ()))
    total = res_ref[...].astype(F32)
    for i in order:
        source = lax.rem(level + planes - i, planes)
        back_keeps[i].wait()
        for j in range(1, plane):
            beside_arrival(*back_args, i, j).wait_recv()
        back = back_recv[source].reshape(group, half)
        mixed = lax.dot_general(
            tables_recv[source, 1], back, over_slots, preferred_element_type=F32
        ) + lax.dot_general(tables_recv[source, 2], back, over_slots, preferred_element_type=F32)
        if i == 0:
            total = total + mixed
        else:
            sum_send[source] = mixed.astype(BF16)
            sum_copy(i).start()
    for i in range(1, planes):
        sum_arrival(i).wait_recv()
        total = total + sum_recv[lax.rem(level + i, planes)].astype(F32)
    out_ref[...] = total.astype(BF16)

    for i in range(1, planes):
        to_column(*table_args, i).wait_send()
        rows_copy(i).wait_send()
        sum_copy(i).wait_send()
    for i in range(planes):
        for j in range(1, plane):
            beside_copy(*disp_args, i, j).wait_send()
            beside_copy(*back_args, i, j).wait_send()


def local(
    tokens,
    norm1_gain,
    w_query,
    w_key,
    w_value,
    head_bias,
    key_cache,
    value_cache,
    seq_lengths,
    w_out,
    norm2_gain,
    route_ids,
    route_logits,
    expert_gate,
    expert_up,
    expert_down,
):
    n = lax.axis_size("ep")
    seqs, half = tokens.shape
    top = route_ids.shape[1]
    experts = n * expert_gate.shape[0]
    capacity = max(2, 2 * seqs * top // experts)
    cap = -(-capacity // 16) * 16
    slots = n * cap
    planes = 4 if n % 4 == 0 else 1
    plane = n // planes
    qc = w_query.shape[1] // 2
    kcols = w_key.shape[1] // 2
    groups = qc // HEAD
    positions = key_cache.shape[1]
    hidden = expert_gate.shape[2]
    tiles = half // COL_BLOCK
    keys = jnp.swapaxes(key_cache, 1, 2)
    values = jnp.swapaxes(value_cache, 1, 2)
    operands = (
        tokens,
        norm1_gain.reshape(1, -1),
        w_query,
        w_key,
        w_value,
        head_bias,
        keys,
        values,
        seq_lengths,
        w_out,
        norm2_gain.reshape(1, -1),
        route_ids.T,
        route_logits.T,
        expert_gate.reshape(expert_gate.shape[1:]),
        expert_up.reshape(expert_up.shape[1:]),
        expert_down.reshape(expert_down.shape[1:]),
    )
    in_smem = (5, 8)
    in_specs = [
        pl.BlockSpec(memory_space=pltpu.SMEM if i in in_smem else pl.ANY)
        for i in range(len(operands))
    ]
    vmem = pl.BlockSpec(memory_space=pltpu.VMEM)
    loaded = [
        pltpu.VMEM(a.shape, a.dtype) for i, a in enumerate(operands) if i not in in_smem
    ]
    dma = pltpu.SemaphoreType.DMA
    scratch = (
        [loaded[0], loaded[0]]
        + loaded[1:]
        + [
            pltpu.VMEM((seqs, qc + 2 * kcols), F32),
            pltpu.VMEM((seqs, qc + 2 * kcols), F32),
            pltpu.VMEM((seqs, groups, HEAD), F32),
            pltpu.VMEM((seqs * groups, positions), F32),
            pltpu.VMEM((seqs, groups, HEAD), F32),
            pltpu.VMEM((2, seqs, half), BF16),
            pltpu.VMEM((2, seqs, half), BF16),
            pltpu.VMEM((seqs, half), BF16),
            pltpu.VMEM((planes, 3, plane * cap, seqs), BF16),
            pltpu.VMEM((planes, 3, plane * cap, seqs), BF16),
            pltpu.VMEM((seqs, half), BF16),
            pltpu.VMEM((planes, seqs, half), BF16),
            pltpu.VMEM((planes, plane, cap, half), BF16),
            pltpu.VMEM((planes, plane, cap, half), BF16),
            pltpu.VMEM((planes, plane, cap, half), BF16),
            pltpu.VMEM((slots, hidden), F32),
            pltpu.VMEM((slots, hidden), F32),
            pltpu.VMEM((slots, hidden), BF16),
            pltpu.VMEM((tiles, slots, COL_BLOCK), BF16),
            pltpu.VMEM((tiles, slots, COL_BLOCK), BF16),
            pltpu.VMEM((tiles, slots, COL_BLOCK), BF16),
            pltpu.VMEM((planes, plane, cap, half), BF16),
            pltpu.VMEM((planes, plane, cap, half), BF16),
            pltpu.VMEM((planes, seqs, half), BF16),
            pltpu.VMEM((planes, seqs, half), BF16),
            dma((len(loaded),)),
            dma((3,)),
            dma((3,)),
            dma((planes,)),
            dma((planes,)),
            dma((planes,)),
            dma((planes,)),
            dma((planes,)),
            dma((planes,)),
            dma((planes, plane)),
            dma((planes, plane)),
            dma((planes, plane)),
            dma((planes, plane)),
            dma((tiles,)),
            dma((tiles,)),
            dma((planes, plane)),
            dma((planes, plane)),
            dma((2 * planes,)),
        ]
    )
    return pl.pallas_call(
        functools.partial(kernel, n, cap),
        out_shape=(
            jax.ShapeDtypeStruct((seqs, half), BF16),
            jax.ShapeDtypeStruct((seqs, kcols), BF16),
            jax.ShapeDtypeStruct((seqs, kcols), BF16),
        ),
        in_specs=in_specs,
        out_specs=(vmem, vmem, vmem),
        scratch_shapes=scratch,
        compiler_params=pltpu.CompilerParams(
            collective_id=0, has_side_effects=True, vmem_limit_bytes=64 * 1024 * 1024 - 65536
        ),
    )(*operands)


def solution(mesh):
    in_specs = (
        P("ep", "tp"),
        P("tp"),
        P("tp", None),
        P("tp", None),
        P("tp", None),
        P("tp"),
        P("ep", None, "tp"),
        P("ep", None, "tp"),
        P("ep"),
        P("tp", None),
        P("tp"),
        P("ep", None),
        P("ep", None),
        P("ep", None, "tp"),
        P("ep", None, "tp"),
        P("ep", "tp", None),
    )
    out_specs = (P("ep", "tp"), P("ep", "tp"), P("ep", "tp"))
    return jax.shard_map(local, mesh=mesh, in_specs=in_specs, out_specs=out_specs, check_vma=False)
```

profile of v0, /device:TPU:0, one launch (start us, length us, event | category | flops | bytes accessed | tf_op | source)
XLA Modules:
  0.0 54.0 jit_solution(753963440305049235)
XLA Ops:
  0.6 49.3 %shard_map.175 = (bf16[32,1024]{1,0:T(8,128)(2,1)}, bf16[32,64]{1,0:T(8,128)(2,1)}, bf16[32,64]{1,0:T(8,128)(2,1)}) custom-call(bf16[32,1024]{1,0:T(8,128)(2,1)} %tok_hbm.1, f32[1,1024]{1,0:T(1,128)} %bitcast.14, bf16[1024,1024]{1,0:T(8,128)(2,1)} %wq_hbm.1, bf16[1024,128]{1,0:T(8,128)(2,1)} %wk_hbm.1, bf16[1024,128]{1,0:T(8,128)(2,1)} %wv_hbm.1, ...), custom_call_target="tpu_custom_call" | custom-call | tf_op jit(solution)/shard_map/pallas_call | solution.py:702
  49.9 1.5 %copy.22 = bf16[32,1024]{1,0:T(8,128)(2,1)} copy(bf16[32,1024]{1,0:T(8,128)(2,1)} %get-tuple-element.6) | data formatting | bytes 131072
  51.4 1.3 %copy.23 = bf16[32,64]{1,0:T(8,128)(2,1)} copy(bf16[32,64]{1,0:T(8,128)(2,1)} %get-tuple-element.7) | data formatting | bytes 8192
  52.7 1.3 %copy.24 = bf16[32,64]{1,0:T(8,128)(2,1)} copy(bf16[32,64]{1,0:T(8,128)(2,1)} %get-tuple-element.8) | data formatting | bytes 8192
where the time goes:
time: 54.3 us; the launch traced here: 54 us
  Pallas kernels  49.3 us (91%)
  local copies, waits for them, and re-layouts  4.06 us (7%)
  between operations  0.65 us (1%)
    pallas_call x1, Pallas kernels, local(): pl.pallas_call(functools.partial(kernel, n, cap), out_shape=(jax.ShapeDty...  49.3 us
    unnamed x3, local copies, waits for them, and re-layouts  4.06 us

commit v1 on v0

--- a/solution.py
+++ b/solution.py
@@ -17,6 +17,10 @@
 DEAD = -1e30
 POS_BLOCK = 256
 COL_BLOCK = 256
+GATE_BLOCK = 512
+PAD = 16
+VMEM_BYTES = 63 * 1024 * 1024
+LANES = 128
 
 
 def dot(a, b):
@@ -158,6 +162,19 @@
     def beside(i):
         return level * plane + lax.rem(spot + i, plane)
 
+    if planes == 4:
+        inner = lax.rem((level + 1) // 2, 2)
+        over = lax.rem(level + 2, 4)
+        across = 3 - level
+        partners = (
+            level,
+            level + 1 - 2 * lax.rem(level, 2),
+            inner * across + (1 - inner) * over,
+            inner * over + (1 - inner) * across,
+        )
+    else:
+        partners = (level,)
+
     def greet_column(i, carry):
         pl.semaphore_signal(barrier, inc=1, device_id=(column(i), tp), device_id_type=MESH)
         return carry
@@ -168,39 +185,46 @@
 
     lax.fori_loop(1, planes, greet_column, 0)
     lax.fori_loop(1, plane, greet_beside, 0)
-    pl.semaphore_wait(barrier, planes + plane - 1)
-
-    loads[0].wait()
-    tok_copy = peer_copy(x_own, x_peer, 0)
-    tok_copy.start()
-    loads[1].wait()
-    for i in (2, 3, 4):
+    for i in (0, 1, 2, 3, 4):
         loads[i].wait()
     for i in (5, 6, 7):
         loads[i].start()
     mine = x_own[...].astype(F32)
-    tok_copy.wait()
-    theirs = x_peer[...].astype(F32)
+    mean_own = jnp.sum(mine, axis=1, keepdims=True) / half
+    centred = mine - mean_own
+    square_own = jnp.sum(centred * centred, axis=1, keepdims=True)
+    gain = g1[...]
+    gain_hi = gain.astype(BF16)
+    gain_lo = (gain - gain_hi.astype(F32)).astype(BF16)
+    pad_row = lax.broadcasted_iota(jnp.int32, (PAD, half), 0)
+    gains = jnp.where(
+        pad_row == 0, gain_hi.astype(F32), jnp.where(pad_row == 1, gain_lo.astype(F32), 0.0)
+    )
+    stacked = jnp.concatenate([centred * gain, gains], axis=0).astype(BF16)
+    pq = dot(stacked, wq[...])
+    pk = dot(stacked, wk[...])
+    pv = dot(stacked, wv[...])
+    qc = pq.shape[1] // 2
+    kcols = pk.shape[1] // 2
+    first = tp == 0
+    used = qc + 2 * kcols
+    proj_send[:, :qc] = jnp.where(first, pq[:, qc:], pq[:, :qc])
+    proj_send[:, qc : qc + kcols] = jnp.where(first, pk[:, kcols:], pk[:, :kcols])
+    proj_send[:, qc + kcols : used] = jnp.where(first, pv[:, kcols:], pv[:, :kcols])
+    proj_send[:seqs, used : used + LANES] = jnp.broadcast_to(mean_own, (seqs, LANES))
+    proj_send[:seqs, used + LANES :] = jnp.broadcast_to(square_own, (seqs, LANES))
+    pl.semaphore_wait(barrier, planes + plane - 1)
+
+    proj_copy = peer_copy(proj_send, proj_recv, 1)
+    proj_copy.start()
+    tok_copy = peer_copy(x_own, x_peer, 0)
+    tok_copy.start()
 
     def stats(a, b):
         total = jnp.sum(a, axis=1, keepdims=True) + jnp.sum(b, axis=1, keepdims=True)
         square = jnp.sum(a * a, axis=1, keepdims=True) + jnp.sum(b * b, axis=1, keepdims=True)
         mean = total / width
         return mean, lax.rsqrt(square / width - mean * mean + LN_EPS)
-
-    mean, scale = stats(mine, theirs)
-    normed = ((mine - mean) * scale * g1[...]).astype(BF16)
-    pq = dot(normed, wq[...])
-    pk = dot(normed, wk[...])
-    pv = dot(normed, wv[...])
-    qc = pq.shape[1] // 2
-    kcols = pk.shape[1] // 2
-    first = tp == 0
-    proj_send[:, :qc] = jnp.where(first, pq[:, qc:], pq[:, :qc])
-    proj_send[:, qc : qc + kcols] = jnp.where(first, pk[:, kcols:], pk[:, :kcols])
-    proj_send[:, qc + kcols :] = jnp.where(first, pv[:, kcols:], pv[:, :kcols])
-    proj_copy = peer_copy(proj_send, proj_recv, 1)
-    proj_copy.start()
 
     for i in (11, 12, 13):
         loads[i].start()
@@ -246,37 +270,48 @@
     own_k = jnp.where(first, pk[:, :kcols], pk[:, kcols:])
     own_v = jnp.where(first, pv[:, :kcols], pv[:, kcols:])
     proj_copy.wait()
-    query = (own_q + proj_recv[:, :qc]).astype(BF16).astype(F32)
-    nk_ref[...] = (own_k + proj_recv[:, qc : qc + kcols]).astype(BF16)
-    nv_ref[...] = (own_v + proj_recv[:, qc + kcols :]).astype(BF16)
+    mean_peer = proj_recv[:seqs, used : used + 1]
+    square_peer = proj_recv[:seqs, used + LANES : used + LANES + 1]
+    apart = (mean_own - mean_peer) * 0.5
+    scale = lax.rsqrt((square_own + square_peer) / width + apart * apart + LN_EPS)
+
+    def joined(own, lo, hi):
+        tilt = (own[seqs : seqs + 1] + own[seqs + 1 : seqs + 2]) - (
+            proj_recv[seqs : seqs + 1, lo:hi] + proj_recv[seqs + 1 : seqs + 2, lo:hi]
+        )
+        return (scale * (own[:seqs] + proj_recv[:seqs, lo:hi] + apart * tilt)).astype(BF16)
+
+    query = joined(own_q, 0, qc).astype(F32)
+    nk_ref[...] = joined(own_k, qc, qc + kcols)
+    nv_ref[...] = joined(own_v, qc + kcols, used)
     for h in range(groups):
         q_rows[:, h, :] = query[:, h * HEAD : (h + 1) * HEAD]
 
-    def to_column(src, dst, sends, recvs, i):
-        to = lax.rem(level + i, planes)
+    def to_level(src, dst, sends, recvs, i):
+        to = partners[i]
         return pltpu.make_async_remote_copy(
             src_ref=src.at[to],
             dst_ref=dst.at[level],
-            send_sem=sends.at[i],
-            recv_sem=recvs.at[i],
-            device_id=(column(i), tp),
-            device_id_type=MESH,
-        )
-
-    def from_column(src, dst, sends, recvs, i):
-        source = lax.rem(level + planes - i, planes)
+            send_sem=sends.at[to],
+            recv_sem=recvs.at[level],
+            device_id=(to * plane + spot, tp),
+            device_id_type=MESH,
+        )
+
+    def from_level(src, dst, sends, recvs, i):
+        source = partners[i]
         return pltpu.make_async_remote_copy(
             src_ref=src.at[source],
             dst_ref=dst.at[source],
-            send_sem=sends.at[i],
-            recv_sem=recvs.at[i],
+            send_sem=sends.at[source],
+            recv_sem=recvs.at[source],
             device_id=(source * plane + spot, tp),
             device_id_type=MESH,
         )
 
     table_args = (tables_send, tables_recv, table_send_sem, table_recv_sem)
     for i in range(1, planes):
-        to_column(*table_args, i).start()
+        to_level(*table_args, i).start()
     tables_recv[level] = tables_send[level]
 
     positions = kc.shape[2]
@@ -344,6 +379,7 @@
     part_copy = peer_copy(part_send, part_recv, 2)
     part_copy.start()
     loads[8].wait()
+    tok_copy.wait()
     part_copy.wait()
     mine = x_own[...].astype(F32)
     theirs = x_peer[...].astype(F32)
@@ -358,28 +394,29 @@
     rows_ref[...] = normed_two
 
     def rows_copy(i):
+        to = partners[i]
         return pltpu.make_async_remote_copy(
             src_ref=rows_ref,
             dst_ref=rows_recv.at[level],
-            send_sem=rows_send_sem.at[i],
-            recv_sem=rows_recv_sem.at[i],
-            device_id=(column(i), tp),
+            send_sem=rows_send_sem.at[to],
+            recv_sem=rows_recv_sem.at[level],
+            device_id=(to * plane + spot, tp),
             device_id_type=MESH,
         )
 
     def rows_arrival(i):
-        source = lax.rem(level + planes - i, planes)
+        source = partners[i]
         return pltpu.make_async_remote_copy(
             src_ref=rows_ref,
             dst_ref=rows_recv.at[source],
-            send_sem=rows_send_sem.at[i],
-            recv_sem=rows_recv_sem.at[i],
+            send_sem=rows_send_sem.at[source],
+            recv_sem=rows_recv_sem.at[source],
             device_id=(source * plane + spot, tp),
             device_id_type=MESH,
         )
 
     def beside_copy(src, dst, sends, recvs, i, j):
-        source = lax.rem(level + planes - i, planes)
+        source = partners[i]
         to = lax.rem(spot + j, plane)
         return pltpu.make_async_remote_copy(
             src_ref=src.at[source, to],
@@ -391,7 +428,7 @@
         )
 
     def beside_arrival(src, dst, sends, recvs, i, j):
-        source = lax.rem(level + planes - i, planes)
+        source = partners[i]
         giver = lax.rem(spot + plane - j, plane)
         return pltpu.make_async_remote_copy(
             src_ref=src.at[source, giver],
@@ -402,14 +439,13 @@
             device_id_type=MESH,
         )
 
-    def fwd_copy(i, j):
-        source = lax.rem(level + planes - i, planes)
-        giver = lax.rem(spot + plane - j, plane)
-        return pltpu.make_async_remote_copy(
-            src_ref=recv_own.at[source, giver],
-            dst_ref=recv_peer.at[source, giver],
-            send_sem=fwd_send_sem.at[i, j],
-            recv_sem=fwd_recv_sem.at[i, j],
+    def fwd_copy(i):
+        source = partners[i]
+        return pltpu.make_async_remote_copy(
+            src_ref=recv_own.at[source],
+            dst_ref=recv_peer.at[source],
+            send_sem=fwd_send_sem.at[i],
+            recv_sem=fwd_recv_sem.at[i],
             device_id=(ep, other),
             device_id_type=MESH,
         )
@@ -418,11 +454,11 @@
     for i in range(1, planes):
         rows_copy(i).start()
     for i in range(1, planes):
-        from_column(*table_args, i).wait_recv()
+        from_level(*table_args, i).wait_recv()
     keeps = []
 
     def place_rows(i, rows):
-        source = lax.rem(level + planes - i, planes)
+        source = partners[i]
         placed = dot(tables_recv[source, 0], rows).astype(BF16)
         disp[source] = placed.reshape(plane, cap, half)
         for j in range(1, plane):
@@ -436,13 +472,12 @@
     place_rows(0, normed_two)
     for i in range(1, planes):
         rows_arrival(i).wait_recv()
-        place_rows(i, rows_recv[lax.rem(level + planes - i, planes)])
+        place_rows(i, rows_recv[partners[i]])
     for i in range(planes):
         keeps[i].wait()
-        fwd_copy(i, 0).start()
         for j in range(1, plane):
             beside_arrival(*disp_args, i, j).wait_recv()
-            fwd_copy(i, j).start()
+        fwd_copy(i).start()
 
     loads[11].wait()
     loads[12].wait()
@@ -452,7 +487,7 @@
     hidden = gate.shape[1]
 
     def first_half(i, carry):
-        cols = pl.ds(pl.multiple_of(i * COL_BLOCK, COL_BLOCK), COL_BLOCK)
+        cols = pl.ds(pl.multiple_of(i * GATE_BLOCK, GATE_BLOCK), GATE_BLOCK)
         depth = pl.ds(pl.multiple_of(tp * half, half), half)
         for r in range(row_blocks):
             rows = recv_own[r * per_block : (r + 1) * per_block].reshape(rows_block, half)
@@ -461,14 +496,13 @@
             up_acc[at, cols] = dot(rows, up[depth, cols])
         return carry
 
-    lax.fori_loop(0, hidden // COL_BLOCK, first_half, 0)
+    lax.fori_loop(0, hidden // GATE_BLOCK, first_half, 0)
 
     for i in range(planes):
-        for j in range(plane):
-            fwd_copy(i, j).wait()
+        fwd_copy(i).wait()
 
     def second_half(i, carry):
-        cols = pl.ds(pl.multiple_of(i * COL_BLOCK, COL_BLOCK), COL_BLOCK)
+        cols = pl.ds(pl.multiple_of(i * GATE_BLOCK, GATE_BLOCK), GATE_BLOCK)
         depth = pl.ds(pl.multiple_of(other * half, half), half)
         for r in range(row_blocks):
             rows = recv_peer[r * per_block : (r + 1) * per_block].reshape(rows_block, half)
@@ -482,7 +516,7 @@
             ).astype(BF16)
         return carry
 
-    lax.fori_loop(0, hidden // COL_BLOCK, second_half, 0)
+    lax.fori_loop(0, hidden // GATE_BLOCK, second_half, 0)
 
     loads[13].wait()
     tiles = half // COL_BLOCK
@@ -523,43 +557,22 @@
         )
 
     back_args = (back_send, back_recv, back_send_sem, back_recv_sem)
-    order = tuple(range(1, planes)) + (0,)
+    order = tuple(reversed(range(planes)))
     back_keeps = {}
     for i in order:
         for j in range(1, plane):
             beside_copy(*back_args, i, j).start()
-        source = lax.rem(level + planes - i, planes)
+        source = partners[i]
         back_keeps[i] = pltpu.make_async_copy(
             back_send.at[source, spot], back_recv.at[source, spot], local_sem.at[planes + i]
         )
         back_keeps[i].start()
 
-    def sum_copy(i):
-        source = lax.rem(level + planes - i, planes)
-        return pltpu.make_async_remote_copy(
-            src_ref=sum_send.at[source],
-            dst_ref=sum_recv.at[level],
-            send_sem=sum_send_sem.at[i],
-            recv_sem=sum_recv_sem.at[i],
-            device_id=(source * plane + spot, tp),
-            device_id_type=MESH,
-        )
-
-    def sum_arrival(i):
-        giver = lax.rem(level + i, planes)
-        return pltpu.make_async_remote_copy(
-            src_ref=sum_send.at[giver],
-            dst_ref=sum_recv.at[giver],
-            send_sem=sum_send_sem.at[i],
-            recv_sem=sum_recv_sem.at[i],
-            device_id=(giver * plane + spot, tp),
-            device_id_type=MESH,
-        )
-
+    sum_args = (sum_send, sum_recv, sum_send_sem, sum_recv_sem)
     over_slots = (((0,), (0,)), ((), ()))
     total = res_ref[...].astype(F32)
     for i in order:
-        source = lax.rem(level + planes - i, planes)
+        source = partners[i]
         back_keeps[i].wait()
         for j in range(1, plane):
             beside_arrival(*back_args, i, j).wait_recv()
@@ -571,20 +584,32 @@
             total = total + mixed
         else:
             sum_send[source] = mixed.astype(BF16)
-            sum_copy(i).start()
+            to_level(*sum_args, i).start()
     for i in range(1, planes):
-        sum_arrival(i).wait_recv()
-        total = total + sum_recv[lax.rem(level + i, planes)].astype(F32)
+        from_level(*sum_args, i).wait_recv()
+        total = total + sum_recv[partners[i]].astype(F32)
     out_ref[...] = total.astype(BF16)
 
     for i in range(1, planes):
-        to_column(*table_args, i).wait_send()
+        to_level(*table_args, i).wait_send()
         rows_copy(i).wait_send()
-        sum_copy(i).wait_send()
+        to_level(*sum_args, i).wait_send()
     for i in range(planes):
         for j in range(1, plane):
             beside_copy(*disp_args, i, j).wait_send()
             beside_copy(*back_args, i, j).wait_send()
+
+
+def publish(*refs):
+    sems = refs[-1]
+    count = len(refs) // 2
+    copies = []
+    for i in range(count):
+        copy = pltpu.make_async_copy(refs[i], refs[count + i], sems.at[i])
+        copy.start()
+        copies.append(copy)
+    for copy in copies:
+        copy.wait()
 
 
 def local(
@@ -654,8 +679,8 @@
         [loaded[0], loaded[0]]
         + loaded[1:]
         + [
-            pltpu.VMEM((seqs, qc + 2 * kcols), F32),
-            pltpu.VMEM((seqs, qc + 2 * kcols), F32),
+            pltpu.VMEM((seqs + PAD, qc + 2 * kcols + 2 * LANES), F32),
+            pltpu.VMEM((seqs + PAD, qc + 2 * kcols + 2 * LANES), F32),
             pltpu.VMEM((seqs, groups, HEAD), F32),
             pltpu.VMEM((seqs * groups, positions), F32),
             pltpu.VMEM((seqs, groups, HEAD), F32),
@@ -690,8 +715,8 @@
             dma((planes,)),
             dma((planes, plane)),
             dma((planes, plane)),
-            dma((planes, plane)),
-            dma((planes, plane)),
+            dma((planes,)),
+            dma((planes,)),
             dma((tiles,)),
             dma((tiles,)),
             dma((planes, plane)),
@@ -699,20 +724,24 @@
             dma((2 * planes,)),
         ]
     )
-    return pl.pallas_call(
+    shapes = ((seqs, half), (seqs, kcols), (seqs, kcols))
+    results = pl.pallas_call(
         functools.partial(kernel, n, cap),
-        out_shape=(
-            jax.ShapeDtypeStruct((seqs, half), BF16),
-            jax.ShapeDtypeStruct((seqs, kcols), BF16),
-            jax.ShapeDtypeStruct((seqs, kcols), BF16),
-        ),
+        out_shape=tuple(pltpu.VMEM(shape, BF16) for shape in shapes),
         in_specs=in_specs,
         out_specs=(vmem, vmem, vmem),
         scratch_shapes=scratch,
         compiler_params=pltpu.CompilerParams(
-            collective_id=0, has_side_effects=True, vmem_limit_bytes=64 * 1024 * 1024 - 65536
+            collective_id=0, has_side_effects=True, vmem_limit_bytes=VMEM_BYTES
         ),
     )(*operands)
+    return pl.pallas_call(
+        publish,
+        out_shape=tuple(jax.ShapeDtypeStruct(shape, BF16) for shape in shapes),
+        in_specs=[vmem] * len(shapes),
+        out_specs=tuple([pl.BlockSpec(memory_space=pl.ANY)] * len(shapes)),
+        scratch_shapes=[dma((len(shapes),))],
+    )(*(pltpu.with_memory_space_constraint(r, pltpu.VMEM) for r in results))
 
 
 def solution(mesh):

time: 54.3 us -> 45.2 us (0.83)
  Pallas kernels: 49.3 us -> 44.4 us
  local copies, waits for them, and re-layouts: 4.06 us -> 0 us
    pallas_call x1 -> x2, Pallas kernels: 49.3 us -> 44.4 us  [the longest x1 43.7 us: local(): pl.pallas_call(functools.partial(kernel, n, cap), out_shape=tuple((pltpu....]
    unnamed x3 -> x0, local copies, waits for them, and re-layouts: 4.06 us -> none
where the time goes in v1:
time: 45.2 us; the launch traced here: 45 us
  Pallas kernels  44.4 us (98%)
  between operations  0.65 us (1%)
    pallas_call x1, Pallas kernels, local(): pl.pallas_call(functools.partial(kernel, n, cap), out_shape=tuple((pltpu....  43.7 us

profile of v1, /device:TPU:0, one launch (start us, length us, event | category | flops | bytes accessed | tf_op | source)
XLA Modules:
  0.0 45.0 jit_solution(2719167435764215096)
XLA Ops:
  0.6 43.7 %shard_map.175 = (bf16[32,1024]{1,0:T(8,128)(2,1)S(1)}, bf16[32,64]{1,0:T(8,128)(2,1)S(1)}, bf16[32,64]{1,0:T(8,128)(2,1)S(1)}) custom-call(bf16[32,1024]{1,0:T(8,128)(2,1)} %tok_hbm.1, f32[1,1024]{1,0:T(1,128)} %bitcast.14, bf16[1024,1024]{1,0:T(8,128)(2,1)} %wq_hbm.1, bf16[1024,128]{1,0:T(8,128)(2,1)} %wk_hbm.1, bf16[1024,128]{1,0:T(8,128)(2,1)} %wv_hbm.1, ...), custom_call_target="tpu_custom_call" | custom-call | tf_op jit(solution)/shard_map/pallas_call | solution.py:728
  44.4 0.7 %shard_map.176 = (bf16[32,1024]{1,0:T(8,128)(2,1)}, bf16[32,64]{1,0:T(8,128)(2,1)}, bf16[32,64]{1,0:T(8,128)(2,1)}) custom-call(bf16[32,1024]{1,0:T(8,128)(2,1)S(1)} %get-tuple-element.6.refs_0_, bf16[32,64]{1,0:T(8,128)(2,1)S(1)} %get-tuple-element.7.refs_1_, bf16[32,64]{1,0:T(8,128)(2,1)S(1)} %get-tuple-element.8.refs_2_), custom_call_target="tpu_custom_call" | custom-call | tf_op jit(solution)/shard_map/pallas_call | solution.py:738

commit v2 on v1

v2 whole, which is shorter than its diff:
```python
import functools

import jax
import jax.numpy as jnp
from jax import lax
from jax.experimental import pallas as pl
from jax.experimental.pallas import tpu as pltpu
from jax.sharding import PartitionSpec as P

HEAD = 64
LN_EPS = 1e-05
SWIGLU_ALPHA = 1.702
SWIGLU_LIMIT = 7.0
MESH = pl.DeviceIdType.MESH
F32 = jnp.float32
BF16 = jnp.bfloat16
DEAD = -1e30
POS_BLOCK = 256
COL_BLOCK = 512
GATE_BLOCK = 512
PAD = 16
BATCH = 4
CHUNKS = 2
VMEM_BYTES = 63 * 1024 * 1024
LANES = 128


def dot(a, b):
    return jnp.dot(a, b, preferred_element_type=F32)


def kernel(
    n,
    cap,
    tok_hbm,
    g1_hbm,
    wq_hbm,
    wk_hbm,
    wv_hbm,
    bias_ref,
    kc_hbm,
    vc_hbm,
    lens_ref,
    wo_hbm,
    g2_hbm,
    ids_hbm,
    logits_hbm,
    gate_hbm,
    up_hbm,
    down_hbm,
    out_ref,
    nk_ref,
    nv_ref,
    x_own,
    x_peer,
    g1,
    wq,
    wk,
    wv,
    kc,
    vc,
    wo,
    g2,
    ids,
    logits,
    gate,
    up,
    down,
    proj_send,
    proj_recv,
    q_rows,
    q_wide,
    z_ref,
    w_ref,
    att_ref,
    part_send,
    part_recv,
    res_ref,
    route_send,
    route_recv,
    tables,
    rows_ref,
    rows_recv,
    disp,
    recv_own,
    recv_peer,
    gate_acc,
    up_acc,
    act_ref,
    down_send,
    down_recv,
    down_own,
    back_send,
    back_recv,
    sum_send,
    sum_recv,
    total_ref,
    load_sem,
    one_send,
    one_recv,
    route_send_sem,
    route_recv_sem,
    rows_send_sem,
    rows_recv_sem,
    sum_send_sem,
    sum_recv_sem,
    disp_send_sem,
    disp_recv_sem,
    fwd_send_sem,
    fwd_recv_sem,
    down_send_sem,
    down_recv_sem,
    back_send_sem,
    back_recv_sem,
    local_sem,
    back_local_sem,
):
    ep = lax.axis_index("ep")
    tp = lax.axis_index("tp")
    other = 1 - tp
    seqs, half = x_own.shape
    width = 2 * half

    loads = []
    pairs = (
        (tok_hbm, x_own),
        (g1_hbm, g1),
        (wq_hbm, wq),
        (wk_hbm, wk),
        (wv_hbm, wv),
        (kc_hbm, kc),
        (vc_hbm, vc),
        (wo_hbm, wo),
        (g2_hbm, g2),
        (ids_hbm, ids),
        (logits_hbm, logits),
        (gate_hbm, gate),
        (up_hbm, up),
        (down_hbm, down),
    )
    for i, (src, dst) in enumerate(pairs):
        copy = pltpu.make_async_copy(src, dst, load_sem.at[i])
        loads.append(copy)
    for i in (0, 2, 3, 4, 1, 9, 10, 8):
        loads[i].start()

    def peer_copy(src, dst, i):
        return pltpu.make_async_remote_copy(
            src_ref=src,
            dst_ref=dst,
            send_sem=one_send.at[i],
            recv_sem=one_recv.at[i],
            device_id=(ep, other),
            device_id_type=MESH,
        )

    barrier = pltpu.get_barrier_semaphore()
    pl.semaphore_signal(barrier, inc=1, device_id=(ep, other), device_id_type=MESH)

    planes = tables.shape[0]
    plane = n // planes
    level = ep // plane
    spot = ep % plane

    def column(i):
        return lax.rem(level + i, planes) * plane + spot

    def beside(i):
        return level * plane + lax.rem(spot + i, plane)

    if planes == 4:
        inner = lax.rem((level + 1) // 2, 2)
        over = lax.rem(level + 2, 4)
        across = 3 - level
        partners = (
            level,
            inner * across + (1 - inner) * over,
            level + 1 - 2 * lax.rem(level, 2),
            inner * over + (1 - inner) * across,
        )
        pairs = ((0, 1), (2, 3))
        eager = (1, 3, 2)
    else:
        partners = (level,)
        pairs = ((0,),)
        eager = ()

    def greet_column(i, carry):
        pl.semaphore_signal(barrier, inc=1, device_id=(column(i), tp), device_id_type=MESH)
        return carry

    def greet_beside(i, carry):
        pl.semaphore_signal(barrier, inc=1, device_id=(beside(i), tp), device_id_type=MESH)
        return carry

    lax.fori_loop(1, planes, greet_column, 0)
    lax.fori_loop(1, plane, greet_beside, 0)
    for i in (0, 1, 2, 3, 4):
        loads[i].wait()
    for i in (5, 6, 7):
        loads[i].start()
    mine = x_own[...].astype(F32)
    mean_own = jnp.sum(mine, axis=1, keepdims=True) / half
    centred = mine - mean_own
    square_own = jnp.sum(centred * centred, axis=1, keepdims=True)
    gain = g1[...]
    gain_hi = gain.astype(BF16)
    gain_lo = (gain - gain_hi.astype(F32)).astype(BF16)
    pad_row = lax.broadcasted_iota(jnp.int32, (PAD, half), 0)
    gains = jnp.where(
        pad_row == 0, gain_hi.astype(F32), jnp.where(pad_row == 1, gain_lo.astype(F32), 0.0)
    )
    stacked = jnp.concatenate([centred * gain, gains], axis=0).astype(BF16)
    pq = dot(stacked, wq[...])
    pk = dot(stacked, wk[...])
    pv = dot(stacked, wv[...])
    qc = pq.shape[1] // 2
    kcols = pk.shape[1] // 2
    first = tp == 0
    used = qc + 2 * kcols
    proj_send[:, :qc] = jnp.where(first, pq[:, qc:], pq[:, :qc])
    proj_send[:, qc : qc + kcols] = jnp.where(first, pk[:, kcols:], pk[:, :kcols])
    proj_send[:, qc + kcols : used] = jnp.where(first, pv[:, kcols:], pv[:, :kcols])
    proj_send[:seqs, used : used + LANES] = jnp.broadcast_to(mean_own, (seqs, LANES))
    proj_send[:seqs, used + LANES :] = jnp.broadcast_to(square_own, (seqs, LANES))
    pl.semaphore_wait(barrier, planes + plane - 1)

    proj_copy = peer_copy(proj_send, proj_recv, 1)
    proj_copy.start()
    loads[9].wait()
    loads[10].wait()
    top = ids.shape[0]
    route_send[:top] = ids[...].astype(F32)
    route_send[top:] = logits[...]

    def route_copy(i, mine):
        to = partners[i]
        return pltpu.make_async_remote_copy(
            src_ref=route_send,
            dst_ref=route_recv.at[level if mine else to],
            send_sem=route_send_sem.at[to],
            recv_sem=route_recv_sem.at[level if mine else to],
            device_id=(to * plane + spot, tp),
            device_id_type=MESH,
        )

    for i in eager:
        route_copy(i, True).start()
    tok_copy = peer_copy(x_own, x_peer, 0)
    tok_copy.start()

    def stats(a, b):
        total = jnp.sum(a, axis=1, keepdims=True) + jnp.sum(b, axis=1, keepdims=True)
        square = jnp.sum(a * a, axis=1, keepdims=True) + jnp.sum(b * b, axis=1, keepdims=True)
        mean = total / width
        return mean, lax.rsqrt(square / width - mean * mean + LN_EPS)

    group = plane * cap
    slot_row = lax.broadcasted_iota(jnp.int32, (group, seqs), 0)
    slot_expert = slot_row // cap
    slot_rank = (slot_row - slot_expert * cap).astype(F32)
    slot_expert = (slot_expert + level * plane).astype(F32)
    earlier = (
        lax.broadcasted_iota(jnp.int32, (seqs, seqs), 0)
        < lax.broadcasted_iota(jnp.int32, (seqs, seqs), 1)
    )
    earlier = jnp.where(earlier, 1.0, 0.0).astype(BF16)

    def make_tables(k):
        route = route_send[...] if k == 0 else route_recv[partners[k]]
        raw = jnp.exp(route[top:])
        probs = raw / jnp.sum(raw, axis=0, keepdims=True)
        hot = jnp.zeros((group, seqs), F32)
        prob_hot = jnp.zeros((group, seqs), F32)
        for i in range(top):
            match = jnp.abs(route[i : i + 1] - slot_expert) < 0.5
            hot = hot + jnp.where(match, 1.0, 0.0)
            prob_hot = prob_hot + jnp.where(match, probs[i : i + 1, :], 0.0)
        rank = dot(hot.astype(BF16), earlier)
        chosen = (hot > 0.5) & (jnp.abs(rank - slot_rank) < 0.5)
        weight = jnp.where(chosen, prob_hot, 0.0)
        weight_hi = weight.astype(BF16)
        tables[k, 0] = jnp.where(chosen, 1.0, 0.0).astype(BF16)
        tables[k, 1] = weight_hi
        tables[k, 2] = (weight - weight_hi.astype(F32)).astype(BF16)

    groups = qc // HEAD
    bias = jnp.zeros((groups, 1), F32)
    head_row = lax.broadcasted_iota(jnp.int32, (groups, 1), 0)
    for h in range(groups):
        bias = bias + jnp.where(head_row == h, bias_ref[h], 0.0)

    own_q = jnp.where(first, pq[:, :qc], pq[:, qc:])
    own_k = jnp.where(first, pk[:, :kcols], pk[:, kcols:])
    own_v = jnp.where(first, pv[:, :kcols], pv[:, kcols:])
    proj_copy.wait()
    mean_peer = proj_recv[:seqs, used : used + 1]
    square_peer = proj_recv[:seqs, used + LANES : used + LANES + 1]
    apart = (mean_own - mean_peer) * 0.5
    scale = lax.rsqrt((square_own + square_peer) / width + apart * apart + LN_EPS)

    def joined(own, lo, hi):
        tilt = (own[seqs : seqs + 1] + own[seqs + 1 : seqs + 2]) - (
            proj_recv[seqs : seqs + 1, lo:hi] + proj_recv[seqs + 1 : seqs + 2, lo:hi]
        )
        return (scale * (own[:seqs] + proj_recv[:seqs, lo:hi] + apart * tilt)).astype(BF16)

    query = joined(own_q, 0, qc).astype(F32)
    nk_ref[...] = joined(own_k, qc, qc + kcols)
    nv_ref[...] = joined(own_v, qc + kcols, used)
    for h in range(groups):
        q_rows[:, h, :] = query[:, h * HEAD : (h + 1) * HEAD]
    flat = q_rows[...].reshape(seqs * groups, HEAD).astype(BF16)
    wide_row = lax.broadcasted_iota(jnp.int32, (seqs * groups, BATCH * HEAD), 0)
    wide_col = lax.broadcasted_iota(jnp.int32, (seqs * groups, BATCH * HEAD), 1)
    q_wide[...] = jnp.where(
        lax.rem(wide_row // groups, BATCH) == wide_col // HEAD,
        jnp.concatenate([flat] * BATCH, axis=1),
        jnp.zeros((), BF16),
    )

    positions = kc.shape[2]
    after = (
        lax.broadcasted_iota(jnp.int32, (POS_BLOCK, POS_BLOCK), 0)
        > lax.broadcasted_iota(jnp.int32, (POS_BLOCK, POS_BLOCK), 1)
    )
    after = jnp.where(after, 1.0, 0.0).astype(BF16)
    chunk = seqs // CHUNKS
    step_rows = BATCH * groups
    place = lax.broadcasted_iota(jnp.int32, (step_rows, positions), 1)
    step_seq = lax.broadcasted_iota(jnp.int32, (step_rows, 1), 0) // groups
    step_bias = jnp.concatenate([bias] * BATCH, axis=0)

    def score(c):
        for i in range(c * chunk // BATCH, (c + 1) * chunk // BATCH):
            rows = slice(i * step_rows, (i + 1) * step_rows)
            keys = kc[i * BATCH : (i + 1) * BATCH].reshape(BATCH * HEAD, positions)
            length = jnp.zeros((step_rows, 1), jnp.int32)
            for j in range(BATCH):
                length = jnp.where(step_seq == j, lens_ref[i * BATCH + j], length)
            s = dot(q_wide[rows, :], keys) * HEAD ** (-0.5) + step_bias
            z_ref[rows, :] = jnp.where(place < length, s, DEAD)

    def spend(c):
        count = chunk * groups
        rows = slice(c * count, (c + 1) * count)
        beyond = jnp.zeros((count, 1), F32)
        for b in reversed(range(positions // POS_BLOCK)):
            cols = slice(b * POS_BLOCK, (b + 1) * POS_BLOCK)
            z = z_ref[rows, cols]
            tail = jnp.log(1.0 + jnp.exp(-jnp.abs(z)))
            spent = jnp.maximum(z, 0.0) + tail
            hi = spent.astype(BF16)
            lo = (spent - hi.astype(F32)).astype(BF16)
            sums = dot(jnp.concatenate([hi, lo], axis=0), after)
            inside = sums[:count] + sums[count:]
            w_ref[rows, cols] = jnp.exp(
                jnp.minimum(z, 0.0) - tail - (inside + beyond)
            ).astype(BF16)
            beyond = beyond + inside[:, :1] + spent[:, :1]

    def read(c):
        for i in range(c * chunk // BATCH, (c + 1) * chunk // BATCH):
            weights = w_ref[i * step_rows : (i + 1) * step_rows, :]
            values = vc[i * BATCH : (i + 1) * BATCH].reshape(BATCH * HEAD, positions)
            mixed = lax.dot_general(
                weights, values, (((1,), (1,)), ((), ())), preferred_element_type=F32
            )
            for j in range(BATCH):
                att_ref[i * BATCH + j] = mixed[
                    j * groups : (j + 1) * groups, j * HEAD : (j + 1) * HEAD
                ]

    def part_copy(c):
        return peer_copy(part_send.at[c], part_recv.at[c], 2 + c)

    def project(c):
        mine = slice(c * chunk, (c + 1) * chunk)
        attended = jnp.concatenate([att_ref[mine, h, :] for h in range(groups)], axis=1)
        part = dot(attended.astype(BF16), wo[...]).astype(BF16)
        part_send[c, 0] = part[:, :half]
        part_send[c, 1] = part[:, half:]
        part_copy(c).start()

    def rows_copy(i, c):
        to = partners[i]
        return pltpu.make_async_remote_copy(
            src_ref=rows_ref.at[c],
            dst_ref=rows_recv.at[level, c],
            send_sem=rows_send_sem.at[to, c],
            recv_sem=rows_recv_sem.at[level, c],
            device_id=(to * plane + spot, tp),
            device_id_type=MESH,
        )

    def rows_arrival(i, c):
        source = partners[i]
        return pltpu.make_async_remote_copy(
            src_ref=rows_ref.at[c],
            dst_ref=rows_recv.at[source, c],
            send_sem=rows_send_sem.at[source, c],
            recv_sem=rows_recv_sem.at[source, c],
            device_id=(source * plane + spot, tp),
            device_id_type=MESH,
        )

    def settle(c):
        at = slice(c * chunk, (c + 1) * chunk)
        part_copy(c).wait()
        res_own = (
            x_own[at, :].astype(F32)
            + (part_send[c, tp].astype(F32) + part_recv[c, tp].astype(F32))
        ).astype(BF16)
        res_other = (
            x_peer[at, :].astype(F32)
            + (part_send[c, other].astype(F32) + part_recv[c, other].astype(F32))
        ).astype(BF16)
        res_ref[at, :] = res_own
        mine = res_own.astype(F32)
        mean, scale = stats(mine, res_other.astype(F32))
        rows_ref[c] = ((mine - mean) * scale * g2[...]).astype(BF16)
        for i in eager:
            rows_copy(i, c).start()

    loads[5].wait()
    for c in range(CHUNKS):
        score(c)
        spend(c)
        if c == 0:
            loads[6].wait()
            for i in (11, 12, 13):
                loads[i].start()
            loads[7].wait()
            loads[8].wait()
            tok_copy.wait()
        else:
            settle(c - 1)
        read(c)
        project(c)
    for k in range(planes):
        if k > 0:
            route_copy(k, False).wait_recv()
        make_tables(k)
    settle(CHUNKS - 1)

    def beside_copy(src, dst, send_sem, recv_sem, j):
        to = lax.rem(spot + j, plane)
        return pltpu.make_async_remote_copy(
            src_ref=src(to),
            dst_ref=dst(spot),
            send_sem=send_sem,
            recv_sem=recv_sem,
            device_id=(level * plane + to, tp),
            device_id_type=MESH,
        )

    def disp_copy(k, j):
        return beside_copy(
            lambda to: disp.at[k, to],
            lambda giver: recv_own.at[k, giver],
            disp_send_sem.at[k],
            disp_recv_sem.at[k],
            j,
        )

    def disp_all(k):
        return pltpu.make_async_remote_copy(
            src_ref=disp.at[k, pl.ds(0, plane - 1)],
            dst_ref=recv_own.at[k, pl.ds(0, plane - 1)],
            send_sem=disp_send_sem.at[k],
            recv_sem=disp_recv_sem.at[k],
            device_id=(ep, other),
            device_id_type=MESH,
        )

    def disp_keep(k):
        return pltpu.make_async_copy(disp.at[k, spot], recv_own.at[k, spot], local_sem.at[k])

    def fwd_copy(k):
        return pltpu.make_async_remote_copy(
            src_ref=recv_own.at[k],
            dst_ref=recv_peer.at[k],
            send_sem=fwd_send_sem.at[k],
            recv_sem=fwd_recv_sem.at[k],
            device_id=(ep, other),
            device_id_type=MESH,
        )

    for k in range(planes):
        if k > 0:
            for c in range(CHUNKS):
                rows_arrival(k, c).wait_recv()
            rows = rows_recv[partners[k]].reshape(seqs, half)
        else:
            rows = rows_ref[...].reshape(seqs, half)
        placed = dot(tables[k, 0], rows).astype(BF16)
        disp[k] = placed.reshape(plane, cap, half)
        for j in range(1, plane):
            disp_copy(k, j).start()
        disp_keep(k).start()

    def gather(k):
        disp_keep(k).wait()
        disp_all(k).wait_recv()
        fwd_copy(k).start()

    hidden = gate.shape[1]
    own_depth = pl.ds(pl.multiple_of(tp * half, half), half)
    peer_depth = pl.ds(pl.multiple_of(other * half, half), half)
    held = len(pairs[0])
    rows_block = min(held * group, 256)
    row_blocks = held * group // rows_block
    per_block = rows_block // cap

    def rows_of(ref, pair, r):
        rows = ref[pair[0] : pair[0] + held].reshape(held * plane, cap, half)
        return rows[r * per_block : (r + 1) * per_block].reshape(rows_block, half)

    def swiglu(g, u):
        c = jnp.minimum(g, SWIGLU_LIMIT)
        linear = jnp.clip(u, -SWIGLU_LIMIT, SWIGLU_LIMIT)
        return (c * jax.nn.sigmoid(SWIGLU_ALPHA * c) * (linear + 1.0)).astype(BF16)

    def first_half(pair):
        def body(i, carry):
            cols = pl.ds(pl.multiple_of(i * GATE_BLOCK, GATE_BLOCK), GATE_BLOCK)
            for r in range(row_blocks):
                rows = rows_of(recv_own, pair, r)
                at = slice(r * rows_block, (r + 1) * rows_block)
                gate_acc[at, cols] = dot(rows, gate[own_depth, cols])
                up_acc[at, cols] = dot(rows, up[own_depth, cols])
            return carry

        lax.fori_loop(0, hidden // GATE_BLOCK, body, 0)

    def second_half(p, pair):
        def body(i, carry):
            cols = pl.ds(pl.multiple_of(i * GATE_BLOCK, GATE_BLOCK), GATE_BLOCK)
            for r in range(row_blocks):
                rows = rows_of(recv_peer, pair, r)
                at = slice(r * rows_block, (r + 1) * rows_block)
                g = gate_acc[at, cols] + dot(rows, gate[peer_depth, cols])
                u = up_acc[at, cols] + dot(rows, up[peer_depth, cols])
                act_ref[p, at, cols] = swiglu(g, u)
            return carry

        lax.fori_loop(0, hidden // GATE_BLOCK, body, 0)

    def whole_depth(p, pair):
        def body(i, carry):
            cols = pl.ds(pl.multiple_of(i * GATE_BLOCK, GATE_BLOCK), GATE_BLOCK)
            for r in range(row_blocks):
                mine = rows_of(recv_own, pair, r)
                theirs = rows_of(recv_peer, pair, r)
                at = slice(r * rows_block, (r + 1) * rows_block)
                g = dot(mine, gate[own_depth, cols]) + dot(theirs, gate[peer_depth, cols])
                u = dot(mine, up[own_depth, cols]) + dot(theirs, up[peer_depth, cols])
                act_ref[p, at, cols] = swiglu(g, u)
            return carry

        lax.fori_loop(0, hidden // GATE_BLOCK, body, 0)

    tiles = half // COL_BLOCK
    all_tiles = pl.ds(0, tiles)
    one_tile = [pl.ds(t, 1) for t in range(tiles)]

    def down_copy(p, t):
        return pltpu.make_async_remote_copy(
            src_ref=down_send.at[p, t],
            dst_ref=down_recv.at[p, t],
            send_sem=down_send_sem.at[p, t],
            recv_sem=down_recv_sem.at[p, t],
            device_id=(ep, other),
            device_id_type=MESH,
        )

    def down_tile(p, side, t, r):
        cols = pl.ds(pl.multiple_of(side * half + t * COL_BLOCK, COL_BLOCK), COL_BLOCK)
        at = slice(r * rows_block, (r + 1) * rows_block)
        return dot(act_ref[p, at, :], down[:, cols]).astype(BF16)

    def down_all(p):
        return pltpu.make_async_remote_copy(
            src_ref=down_send.at[p],
            dst_ref=down_recv.at[p],
            send_sem=down_send_sem.at[p, 0],
            recv_sem=down_recv_sem.at[p, 0],
            device_id=(ep, other),
            device_id_type=MESH,
        )

    def down_other(p, together):
        for t in range(tiles):
            for r in range(row_blocks):
                at = slice(r * rows_block, (r + 1) * rows_block)
                down_send[p, t, at, :] = down_tile(p, other, t, r)
            if not together:
                down_copy(p, t).start()
        if together:
            down_all(p).start()

    def back_copy(k, at, j):
        return beside_copy(
            lambda to: back_send.at[k, to, at],
            lambda giver: back_recv.at[k, giver, at],
            back_send_sem.at[k],
            back_recv_sem.at[k, at.start // at.size],
            j,
        )

    def back_all(k, at):
        return pltpu.make_async_remote_copy(
            src_ref=back_send.at[k, pl.ds(0, plane - 1), at],
            dst_ref=back_recv.at[k, pl.ds(0, plane - 1), at],
            send_sem=back_send_sem.at[k],
            recv_sem=back_recv_sem.at[k, at.start // at.size],
            device_id=(ep, other),
            device_id_type=MESH,
        )

    def back_keep(k, at):
        return pltpu.make_async_copy(
            back_send.at[k, spot, at],
            back_recv.at[k, spot, at],
            back_local_sem.at[k, at.start // at.size],
        )

    def send_back(k, at):
        for j in range(1, plane):
            back_copy(k, at, j).start()
        back_keep(k, at).start()

    def down_join(p, pair, t):
        total = (down_own[t].astype(F32) + down_recv[p, t].astype(F32)).astype(BF16)
        total = total.reshape(held, plane, cap, COL_BLOCK)
        for i, k in enumerate(pair):
            back_send[k, :, t] = total[i]

    def down_mine(p, pair, together):
        for t in range(tiles):
            for r in range(row_blocks):
                at = slice(r * rows_block, (r + 1) * rows_block)
                down_own[t, at, :] = down_tile(p, tp, t, r)
            if not together:
                down_copy(p, t).wait()
                down_join(p, pair, t)
                send_back(pair[-1], one_tile[t])
        if together:
            down_all(p).wait()
            for t in range(tiles):
                down_join(p, pair, t)
            for k in reversed(pair):
                send_back(k, all_tiles)
        else:
            for k in reversed(pair[:-1]):
                for t in range(tiles):
                    send_back(k, one_tile[t])

    def sum_copy(k, t):
        to = partners[k]
        return pltpu.make_async_remote_copy(
            src_ref=sum_send.at[to, t],
            dst_ref=sum_recv.at[level, t],
            send_sem=sum_send_sem.at[to, t],
            recv_sem=sum_recv_sem.at[level, t],
            device_id=(to * plane + spot, tp),
            device_id_type=MESH,
        )

    def sum_arrival(k, t):
        source = partners[k]
        return pltpu.make_async_remote_copy(
            src_ref=sum_send.at[source, t],
            dst_ref=sum_recv.at[source, t],
            send_sem=sum_send_sem.at[source, t],
            recv_sem=sum_recv_sem.at[source, t],
            device_id=(source * plane + spot, tp),
            device_id_type=MESH,
        )

    over_slots = (((0,), (0,)), ((), ()))

    def combine(k, at):
        back_keep(k, at).wait()
        back_all(k, at).wait_recv()
        to = partners[k]
        mixes = []
        for t in range(at.start, at.start + at.size):
            back = back_recv[k, :, t].reshape(group, COL_BLOCK)
            mixes.append(
                lax.dot_general(tables[k, 1], back, over_slots, preferred_element_type=F32)
                + lax.dot_general(tables[k, 2], back, over_slots, preferred_element_type=F32)
            )
        for t, mixed in zip(range(at.start, at.start + at.size), mixes):
            cols = slice(t * COL_BLOCK, (t + 1) * COL_BLOCK)
            if k == 0:
                total_ref[:, cols] = res_ref[:, cols].astype(F32) + mixed
            else:
                sum_send[to, t] = mixed.astype(BF16)
        if k > 0:
            for t in range(at.start, at.start + at.size):
                sum_copy(k, t).start()

    for k in pairs[0]:
        gather(k)
    loads[11].wait()
    loads[12].wait()
    first_half(pairs[0])
    for k in pairs[0]:
        fwd_copy(k).wait()
    second_half(0, pairs[0])
    loads[13].wait()
    down_other(0, True)
    if len(pairs) > 1:
        for k in pairs[1]:
            gather(k)
    down_mine(0, pairs[0], True)
    if len(pairs) > 1:
        for k in pairs[1]:
            fwd_copy(k).wait()
        whole_depth(1, pairs[1])
        down_other(1, False)
        down_mine(1, pairs[1], False)
    for i in range(1, planes):
        route_copy(i, True).wait_send()
        for c in range(CHUNKS):
            rows_copy(i, c).wait_send()
    for k in range(planes):
        disp_all(k).wait_send()
    for k in reversed(pairs[0]):
        combine(k, all_tiles)
        back_all(k, all_tiles).wait_send()
    if len(pairs) > 1:
        for k in reversed(pairs[1]):
            for t in range(tiles):
                combine(k, one_tile[t])
        for k in pairs[1]:
            back_all(k, all_tiles).wait_send()
    for k in eager:
        for t in range(tiles):
            sum_arrival(k, t).wait_recv()
    for t in range(tiles):
        cols = slice(t * COL_BLOCK, (t + 1) * COL_BLOCK)
        total = total_ref[:, cols]
        for k in range(1, planes):
            total = total + sum_recv[partners[k], t].astype(F32)
        out_ref[:, cols] = total.astype(BF16)

    for i in range(1, planes):
        for t in range(tiles):
            sum_copy(i, t).wait_send()


def publish(*refs):
    sems = refs[-1]
    count = len(refs) // 2
    copies = []
    for i in range(count):
        copy = pltpu.make_async_copy(refs[i], refs[count + i], sems.at[i])
        copy.start()
        copies.append(copy)
    for copy in copies:
        copy.wait()


def local(
    tokens,
    norm1_gain,
    w_query,
    w_key,
    w_value,
    head_bias,
    key_cache,
    value_cache,
    seq_lengths,
    w_out,
    norm2_gain,
    route_ids,
    route_logits,
    expert_gate,
    expert_up,
    expert_down,
):
    n = lax.axis_size("ep")
    seqs, half = tokens.shape
    top = route_ids.shape[1]
    experts = n * expert_gate.shape[0]
    capacity = max(2, 2 * seqs * top // experts)
    cap = -(-capacity // 16) * 16
    slots = n * cap
    planes = 4 if n % 4 == 0 else 1
    plane = n // planes
    qc = w_query.shape[1] // 2
    kcols = w_key.shape[1] // 2
    groups = qc // HEAD
    positions = key_cache.shape[1]
    hidden = expert_gate.shape[2]
    tiles = half // COL_BLOCK
    pair_count = 2 if planes == 4 else 1
    keys = jnp.swapaxes(key_cache, 1, 2)
    values = jnp.swapaxes(value_cache, 1, 2)
    operands = (
        tokens,
        norm1_gain.reshape(1, -1),
        w_query,
        w_key,
        w_value,
        head_bias,
        keys,
        values,
        seq_lengths,
        w_out,
        norm2_gain.reshape(1, -1),
        route_ids.T,
        route_logits.T,
        expert_gate.reshape(expert_gate.shape[1:]),
        expert_up.reshape(expert_up.shape[1:]),
        expert_down.reshape(expert_down.shape[1:]),
    )
    in_smem = (5, 8)
    in_specs = [
        pl.BlockSpec(memory_space=pltpu.SMEM if i in in_smem else pl.ANY)
        for i in range(len(operands))
    ]
    vmem = pl.BlockSpec(memory_space=pltpu.VMEM)
    loaded = [
        pltpu.VMEM(a.shape, a.dtype) for i, a in enumerate(operands) if i not in in_smem
    ]
    dma = pltpu.SemaphoreType.DMA
    scratch = (
        [loaded[0], loaded[0]]
        + loaded[1:]
        + [
            pltpu.VMEM((seqs + PAD, qc + 2 * kcols + 2 * LANES), F32),
            pltpu.VMEM((seqs + PAD, qc + 2 * kcols + 2 * LANES), F32),
            pltpu.VMEM((seqs, groups, HEAD), F32),
            pltpu.VMEM((seqs * groups, BATCH * HEAD), BF16),
            pltpu.VMEM((seqs * groups, positions), F32),
            pltpu.VMEM((seqs * groups, positions), BF16),
            pltpu.VMEM((seqs, groups, HEAD), F32),
            pltpu.VMEM((CHUNKS, 2, seqs // CHUNKS, half), BF16),
            pltpu.VMEM((CHUNKS, 2, seqs // CHUNKS, half), BF16),
            pltpu.VMEM((seqs, half), BF16),
            pltpu.VMEM((2 * top, seqs), F32),
            pltpu.VMEM((planes, 2 * top, seqs), F32),
            pltpu.VMEM((planes, 3, plane * cap, seqs), BF16),
            pltpu.VMEM((CHUNKS, seqs // CHUNKS, half), BF16),
            pltpu.VMEM((planes, CHUNKS, seqs // CHUNKS, half), BF16),
            pltpu.VMEM((planes, plane, cap, half), BF16),
            pltpu.VMEM((planes, plane, cap, half), BF16),
            pltpu.VMEM((planes, plane, cap, half), BF16),
            pltpu.VMEM((slots // pair_count, hidden), F32),
            pltpu.VMEM((slots // pair_count, hidden), F32),
            pltpu.VMEM((pair_count, slots // pair_count, hidden), BF16),
            pltpu.VMEM((pair_count, tiles, slots // pair_count, COL_BLOCK), BF16),
            pltpu.VMEM((pair_count, tiles, slots // pair_count, COL_BLOCK), BF16),
            pltpu.VMEM((tiles, slots // pair_count, COL_BLOCK), BF16),
            pltpu.VMEM((planes, plane, tiles, cap, COL_BLOCK), BF16),
            pltpu.VMEM((planes, plane, tiles, cap, COL_BLOCK), BF16),
            pltpu.VMEM((planes, tiles, seqs, COL_BLOCK), BF16),
            pltpu.VMEM((planes, tiles, seqs, COL_BLOCK), BF16),
            pltpu.VMEM((seqs, half), F32),
            dma((len(loaded),)),
            dma((2 + CHUNKS,)),
            dma((2 + CHUNKS,)),
            dma((planes,)),
            dma((planes,)),
            dma((planes, CHUNKS)),
            dma((planes, CHUNKS)),
            dma((planes, tiles)),
            dma((planes, tiles)),
            dma((planes,)),
            dma((planes,)),
            dma((planes,)),
            dma((planes,)),
            dma((pair_count, tiles)),
            dma((pair_count, tiles)),
            dma((planes,)),
            dma((planes, tiles)),
            dma((planes,)),
            dma((planes, tiles)),
        ]
    )
    shapes = ((seqs, half), (seqs, kcols), (seqs, kcols))
    results = pl.pallas_call(
        functools.partial(kernel, n, cap),
        out_shape=tuple(pltpu.VMEM(shape, BF16) for shape in shapes),
        in_specs=in_specs,
        out_specs=(vmem, vmem, vmem),
        scratch_shapes=scratch,
        compiler_params=pltpu.CompilerParams(
            collective_id=0, has_side_effects=True, vmem_limit_bytes=VMEM_BYTES
        ),
    )(*operands)
    return pl.pallas_call(
        publish,
        out_shape=tuple(jax.ShapeDtypeStruct(shape, BF16) for shape in shapes),
        in_specs=[vmem] * len(shapes),
        out_specs=tuple([pl.BlockSpec(memory_space=pl.ANY)] * len(shapes)),
        scratch_shapes=[dma((len(shapes),))],
    )(*(pltpu.with_memory_space_constraint(r, pltpu.VMEM) for r in results))


def solution(mesh):
    in_specs = (
        P("ep", "tp"),
        P("tp"),
        P("tp", None),
        P("tp", None),
        P("tp", None),
        P("tp"),
        P("ep", None, "tp"),
        P("ep", None, "tp"),
        P("ep"),
        P("tp", None),
        P("tp"),
        P("ep", None),
        P("ep", None),
        P("ep", None, "tp"),
        P("ep", None, "tp"),
        P("ep", "tp", None),
    )
    out_specs = (P("ep", "tp"), P("ep", "tp"), P("ep", "tp"))
    return jax.shard_map(local, mesh=mesh, in_specs=in_specs, out_specs=out_specs, check_vma=False)
```

time: 45.2 us -> 43 us (0.951)
  Pallas kernels: 44.4 us -> 42.2 us
    pallas_call x1, Pallas kernels: 43.7 us -> 41.5 us  [local(): pl.pallas_call(functools.partial(kernel, n, cap), out_shape=tuple((pltpu....]
where the time goes in v2:
time: 43 us; the launch traced here: 42.8 us
  Pallas kernels  42.2 us (98%)
  between operations  0.65 us (2%)
    pallas_call x1, Pallas kernels, local(): pl.pallas_call(functools.partial(kernel, n, cap), out_shape=tuple((pltpu....  41.5 us

profile of v2, /device:TPU:0, one launch (start us, length us, event | category | flops | bytes accessed | tf_op | source)
XLA Modules:
  0.0 42.8 jit_solution(17447984065987692421)
XLA Ops:
  0.6 41.5 %shard_map.175 = (bf16[32,1024]{1,0:T(8,128)(2,1)S(1)}, bf16[32,64]{1,0:T(8,128)(2,1)S(1)}, bf16[32,64]{1,0:T(8,128)(2,1)S(1)}) custom-call(bf16[32,1024]{1,0:T(8,128)(2,1)} %tok_hbm.1, f32[1,1024]{1,0:T(1,128)} %bitcast.14, bf16[1024,1024]{1,0:T(8,128)(2,1)} %wq_hbm.1, bf16[1024,128]{1,0:T(8,128)(2,1)} %wk_hbm.1, bf16[1024,128]{1,0:T(8,128)(2,1)} %wv_hbm.1, ...), custom_call_target="tpu_custom_call" | custom-call | tf_op jit(solution)/shard_map/pallas_call | solution.py:885
  42.2 0.7 %shard_map.176 = (bf16[32,1024]{1,0:T(8,128)(2,1)}, bf16[32,64]{1,0:T(8,128)(2,1)}, bf16[32,64]{1,0:T(8,128)(2,1)}) custom-call(bf16[32,1024]{1,0:T(8,128)(2,1)S(1)} %get-tuple-element.6.refs_0_, bf16[32,64]{1,0:T(8,128)(2,1)S(1)} %get-tuple-element.7.refs_1_, bf16[32,64]{1,0:T(8,128)(2,1)S(1)} %get-tuple-element.8.refs_2_), custom_call_target="tpu_custom_call" | custom-call | tf_op jit(solution)/shard_map/pallas_call | solution.py:895

commit v3 on v2

--- a/solution.py
+++ b/solution.py
@@ -37,10 +37,10 @@
     wq_hbm,
     wk_hbm,
     wv_hbm,
-    bias_ref,
+    bias_hbm,
     kc_hbm,
     vc_hbm,
-    lens_ref,
+    lens_hbm,
     wo_hbm,
     g2_hbm,
     ids_hbm,
@@ -51,6 +51,8 @@
     out_ref,
     nk_ref,
     nv_ref,
+    bias_ref,
+    lens_ref,
     x_own,
     x_peer,
     g1,
@@ -102,6 +104,7 @@
     route_recv_sem,
     rows_send_sem,
     rows_recv_sem,
+    relay_sem,
     sum_send_sem,
     sum_recv_sem,
     disp_send_sem,
@@ -137,11 +140,13 @@
         (gate_hbm, gate),
         (up_hbm, up),
         (down_hbm, down),
+        (bias_hbm, bias_ref),
+        (lens_hbm, lens_ref),
     )
     for i, (src, dst) in enumerate(pairs):
         copy = pltpu.make_async_copy(src, dst, load_sem.at[i])
         loads.append(copy)
-    for i in (0, 2, 3, 4, 1, 9, 10, 8):
+    for i in (0, 1, 2, 3, 4, 14, 15, 9, 10, 8, 5, 6, 7):
         loads[i].start()
 
     def peer_copy(src, dst, i):
@@ -170,19 +175,18 @@
 
     if planes == 4:
         inner = lax.rem((level + 1) // 2, 2)
-        over = lax.rem(level + 2, 4)
-        across = 3 - level
         partners = (
             level,
-            inner * across + (1 - inner) * over,
+            lax.rem(level + 2, 4),
             level + 1 - 2 * lax.rem(level, 2),
-            inner * over + (1 - inner) * across,
-        )
-        pairs = ((0, 1), (2, 3))
+            3 - level,
+        )
+        teams = ((0,), (1,), (2, 3))
         eager = (1, 3, 2)
     else:
         partners = (level,)
-        pairs = ((0,),)
+        inner = 0
+        teams = ((0,),)
         eager = ()
 
     def greet_column(i, carry):
@@ -195,10 +199,8 @@
 
     lax.fori_loop(1, planes, greet_column, 0)
     lax.fori_loop(1, plane, greet_beside, 0)
-    for i in (0, 1, 2, 3, 4):
-        loads[i].wait()
-    for i in (5, 6, 7):
-        loads[i].start()
+    loads[0].wait()
+    loads[1].wait()
     mine = x_own[...].astype(F32)
     mean_own = jnp.sum(mine, axis=1, keepdims=True) / half
     centred = mine - mean_own
@@ -211,6 +213,8 @@
         pad_row == 0, gain_hi.astype(F32), jnp.where(pad_row == 1, gain_lo.astype(F32), 0.0)
     )
     stacked = jnp.concatenate([centred * gain, gains], axis=0).astype(BF16)
+    for i in (2, 3, 4):
+        loads[i].wait()
     pq = dot(stacked, wq[...])
     pk = dot(stacked, wk[...])
     pv = dot(stacked, wv[...])
@@ -285,6 +289,8 @@
         tables[k, 2] = (weight - weight_hi.astype(F32)).astype(BF16)
 
     groups = qc // HEAD
+    loads[14].wait()
+    loads[15].wait()
     bias = jnp.zeros((groups, 1), F32)
     head_row = lax.broadcasted_iota(jnp.int32, (groups, 1), 0)
     for h in range(groups):
@@ -382,14 +388,24 @@
         part_send[c, 1] = part[:, half:]
         part_copy(c).start()
 
-    def rows_copy(i, c):
-        to = partners[i]
+    def rows_copy(to, c):
         return pltpu.make_async_remote_copy(
             src_ref=rows_ref.at[c],
             dst_ref=rows_recv.at[level, c],
             send_sem=rows_send_sem.at[to, c],
             recv_sem=rows_recv_sem.at[level, c],
             device_id=(to * plane + spot, tp),
+            device_id_type=MESH,
+        )
+
+    def relay_copy(c):
+        far = partners[1]
+        return pltpu.make_async_remote_copy(
+            src_ref=rows_recv.at[far, c],
+            dst_ref=rows_recv.at[far, c],
+            send_sem=relay_sem.at[c],
+            recv_sem=rows_recv_sem.at[far, c],
+            device_id=(partners[2] * plane + spot, tp),
             device_id_type=MESH,
         )
 
@@ -419,8 +435,14 @@
         mine = res_own.astype(F32)
         mean, scale = stats(mine, res_other.astype(F32))
         rows_ref[c] = ((mine - mean) * scale * g2[...]).astype(BF16)
-        for i in eager:
-            rows_copy(i, c).start()
+        if planes > 1:
+            rows_copy(partners[1], c).start()
+
+            @pl.when(inner == 1)
+            def _():
+                rows_copy(partners[3], c).start()
+
+            rows_copy(partners[2], c).start()
 
     loads[5].wait()
     for c in range(CHUNKS):
@@ -486,10 +508,8 @@
             device_id_type=MESH,
         )
 
-    for k in range(planes):
+    def place_rows(k):
         if k > 0:
-            for c in range(CHUNKS):
-                rows_arrival(k, c).wait_recv()
             rows = rows_recv[partners[k]].reshape(seqs, half)
         else:
             rows = rows_ref[...].reshape(seqs, half)
@@ -499,6 +519,10 @@
             disp_copy(k, j).start()
         disp_keep(k).start()
 
+    def receive_rows(k):
+        for c in range(CHUNKS):
+            rows_arrival(k, c).wait_recv()
+
     def gather(k):
         disp_keep(k).wait()
         disp_all(k).wait_recv()
@@ -507,55 +531,52 @@
     hidden = gate.shape[1]
     own_depth = pl.ds(pl.multiple_of(tp * half, half), half)
     peer_depth = pl.ds(pl.multiple_of(other * half, half), half)
-    held = len(pairs[0])
-    rows_block = min(held * group, 256)
-    row_blocks = held * group // rows_block
-    per_block = rows_block // cap
-
-    def rows_of(ref, pair, r):
-        rows = ref[pair[0] : pair[0] + held].reshape(held * plane, cap, half)
-        return rows[r * per_block : (r + 1) * per_block].reshape(rows_block, half)
+    def blocks_of(team):
+        count = len(team) * group
+        size = min(count, 256)
+        return [slice(i * size, (i + 1) * size) for i in range(count // size)]
+
+    def rows_of(ref, team, at):
+        rows = ref[team[0] : team[-1] + 1].reshape(len(team) * plane, cap, half)
+        return rows[at.start // cap : at.stop // cap].reshape(at.stop - at.start, half)
 
     def swiglu(g, u):
         c = jnp.minimum(g, SWIGLU_LIMIT)
         linear = jnp.clip(u, -SWIGLU_LIMIT, SWIGLU_LIMIT)
         return (c * jax.nn.sigmoid(SWIGLU_ALPHA * c) * (linear + 1.0)).astype(BF16)
 
-    def first_half(pair):
+    def first_half(team):
         def body(i, carry):
             cols = pl.ds(pl.multiple_of(i * GATE_BLOCK, GATE_BLOCK), GATE_BLOCK)
-            for r in range(row_blocks):
-                rows = rows_of(recv_own, pair, r)
-                at = slice(r * rows_block, (r + 1) * rows_block)
+            for at in blocks_of(team):
+                rows = rows_of(recv_own, team, at)
                 gate_acc[at, cols] = dot(rows, gate[own_depth, cols])
                 up_acc[at, cols] = dot(rows, up[own_depth, cols])
             return carry
 
         lax.fori_loop(0, hidden // GATE_BLOCK, body, 0)
 
-    def second_half(p, pair):
+    def second_half(team):
         def body(i, carry):
             cols = pl.ds(pl.multiple_of(i * GATE_BLOCK, GATE_BLOCK), GATE_BLOCK)
-            for r in range(row_blocks):
-                rows = rows_of(recv_peer, pair, r)
-                at = slice(r * rows_block, (r + 1) * rows_block)
+            for at in blocks_of(team):
+                rows = rows_of(recv_peer, team, at)
                 g = gate_acc[at, cols] + dot(rows, gate[peer_depth, cols])
                 u = up_acc[at, cols] + dot(rows, up[peer_depth, cols])
-                act_ref[p, at, cols] = swiglu(g, u)
+                act_ref[at, cols] = swiglu(g, u)
             return carry
 
         lax.fori_loop(0, hidden // GATE_BLOCK, body, 0)
 
-    def whole_depth(p, pair):
+    def whole_depth(team):
         def body(i, carry):
             cols = pl.ds(pl.multiple_of(i * GATE_BLOCK, GATE_BLOCK), GATE_BLOCK)
-            for r in range(row_blocks):
-                mine = rows_of(recv_own, pair, r)
-                theirs = rows_of(recv_peer, pair, r)
-                at = slice(r * rows_block, (r + 1) * rows_block)
+            for at in blocks_of(team):
+                mine = rows_of(recv_own, team, at)
+                theirs = rows_of(recv_peer, team, at)
                 g = dot(mine, gate[own_depth, cols]) + dot(theirs, gate[peer_depth, cols])
                 u = dot(mine, up[own_depth, cols]) + dot(theirs, up[peer_depth, cols])
-                act_ref[p, at, cols] = swiglu(g, u)
+                act_ref[at, cols] = swiglu(g, u)
             return carry
 
         lax.fori_loop(0, hidden // GATE_BLOCK, body, 0)
@@ -564,40 +585,36 @@
     all_tiles = pl.ds(0, tiles)
     one_tile = [pl.ds(t, 1) for t in range(tiles)]
 
-    def down_copy(p, t):
-        return pltpu.make_async_remote_copy(
-            src_ref=down_send.at[p, t],
-            dst_ref=down_recv.at[p, t],
-            send_sem=down_send_sem.at[p, t],
-            recv_sem=down_recv_sem.at[p, t],
+    def down_copy(p, at):
+        team = teams[p]
+        ks = pl.ds(team[0], len(team))
+        return pltpu.make_async_remote_copy(
+            src_ref=down_send.at[at, ks],
+            dst_ref=down_recv.at[at, ks],
+            send_sem=down_send_sem.at[p, at.start // at.size],
+            recv_sem=down_recv_sem.at[p, at.start // at.size],
             device_id=(ep, other),
             device_id_type=MESH,
         )
 
-    def down_tile(p, side, t, r):
+    def down_tile(ref, p, side, t):
+        team = teams[p]
         cols = pl.ds(pl.multiple_of(side * half + t * COL_BLOCK, COL_BLOCK), COL_BLOCK)
-        at = slice(r * rows_block, (r + 1) * rows_block)
-        return dot(act_ref[p, at, :], down[:, cols]).astype(BF16)
-
-    def down_all(p):
-        return pltpu.make_async_remote_copy(
-            src_ref=down_send.at[p],
-            dst_ref=down_recv.at[p],
-            send_sem=down_send_sem.at[p, 0],
-            recv_sem=down_recv_sem.at[p, 0],
-            device_id=(ep, other),
-            device_id_type=MESH,
-        )
-
-    def down_other(p, together):
-        for t in range(tiles):
-            for r in range(row_blocks):
-                at = slice(r * rows_block, (r + 1) * rows_block)
-                down_send[p, t, at, :] = down_tile(p, other, t, r)
-            if not together:
-                down_copy(p, t).start()
-        if together:
-            down_all(p).start()
+        for at in blocks_of(team):
+            value = dot(act_ref[at, :], down[:, cols]).astype(BF16)
+            size = at.stop - at.start
+            if size <= group:
+                k, begin = team[0] + at.start // group, at.start % group
+                ref[t, k, begin : begin + size, :] = value
+            else:
+                k = team[0] + at.start // group
+                ref[t, k : k + size // group] = value.reshape(size // group, group, COL_BLOCK)
+
+    def down_other(p, parts):
+        for at in parts:
+            for t in range(at.start, at.start + at.size):
+                down_tile(down_send, p, other, t)
+            down_copy(p, at).start()
 
     def back_copy(k, at, j):
         return beside_copy(
@@ -630,31 +647,31 @@
             back_copy(k, at, j).start()
         back_keep(k, at).start()
 
-    def down_join(p, pair, t):
-        total = (down_own[t].astype(F32) + down_recv[p, t].astype(F32)).astype(BF16)
-        total = total.reshape(held, plane, cap, COL_BLOCK)
-        for i, k in enumerate(pair):
-            back_send[k, :, t] = total[i]
-
-    def down_mine(p, pair, together):
+    def down_join(p, t):
+        for k in teams[p]:
+            total = (down_own[t, k].astype(F32) + down_recv[t, k].astype(F32)).astype(BF16)
+            back_send[k, :, t] = total.reshape(plane, cap, COL_BLOCK)
+
+    def down_mine(p):
         for t in range(tiles):
-            for r in range(row_blocks):
-                at = slice(r * rows_block, (r + 1) * rows_block)
-                down_own[t, at, :] = down_tile(p, tp, t, r)
-            if not together:
-                down_copy(p, t).wait()
-                down_join(p, pair, t)
-                send_back(pair[-1], one_tile[t])
-        if together:
-            down_all(p).wait()
+            down_tile(down_own, p, tp, t)
+
+    def join_whole(p):
+        down_copy(p, all_tiles).wait()
+        for t in range(tiles):
+            down_join(p, t)
+        for k in teams[p]:
+            send_back(k, all_tiles)
+
+    def join_tiles(p):
+        for t in range(tiles):
+            down_tile(down_own, p, tp, t)
+            down_copy(p, one_tile[t]).wait()
+            down_join(p, t)
+            send_back(teams[p][-1], one_tile[t])
+        for k in reversed(teams[p][:-1]):
             for t in range(tiles):
-                down_join(p, pair, t)
-            for k in reversed(pair):
-                send_back(k, all_tiles)
-        else:
-            for k in reversed(pair[:-1]):
-                for t in range(tiles):
-                    send_back(k, one_tile[t])
+                send_back(k, one_tile[t])
 
     def sum_copy(k, t):
         to = partners[k]
@@ -701,40 +718,70 @@
             for t in range(at.start, at.start + at.size):
                 sum_copy(k, t).start()
 
-    for k in pairs[0]:
-        gather(k)
-    loads[11].wait()
-    loads[12].wait()
-    first_half(pairs[0])
-    for k in pairs[0]:
-        fwd_copy(k).wait()
-    second_half(0, pairs[0])
-    loads[13].wait()
-    down_other(0, True)
-    if len(pairs) > 1:
-        for k in pairs[1]:
-            gather(k)
-    down_mine(0, pairs[0], True)
-    if len(pairs) > 1:
-        for k in pairs[1]:
-            fwd_copy(k).wait()
-        whole_depth(1, pairs[1])
-        down_other(1, False)
-        down_mine(1, pairs[1], False)
-    for i in range(1, planes):
-        route_copy(i, True).wait_send()
+    def run_far():
+        whole_depth(teams[2])
+        down_other(2, one_tile)
+        join_tiles(2)
+
+    place_rows(0)
+    if planes > 1:
+        receive_rows(1)
+
+        @pl.when(inner == 1)
+        def _():
+            for c in range(CHUNKS):
+                relay_copy(c).start()
+
+        place_rows(1)
+    gather(0)
+    if planes > 1:
+        receive_rows(2)
+        place_rows(2)
+    for i in (11, 12, 13):
+        loads[i].wait()
+    fwd_copy(0).wait()
+    whole_depth(teams[0])
+    down_other(0, [all_tiles])
+    if planes > 1:
+        receive_rows(3)
+        place_rows(3)
+    down_mine(0)
+    join_whole(0)
+    if planes > 1:
+        gather(1)
+        first_half(teams[1])
+        fwd_copy(1).wait()
+        second_half(teams[1])
+        down_other(1, [all_tiles])
+        gather(2)
+        gather(3)
+        down_mine(1)
+        join_whole(1)
+        fwd_copy(2).wait()
+        fwd_copy(3).wait()
+        run_far()
+        for i in range(1, planes):
+            route_copy(i, True).wait_send()
         for c in range(CHUNKS):
-            rows_copy(i, c).wait_send()
+            rows_copy(partners[1], c).wait_send()
+            rows_copy(partners[2], c).wait_send()
+
+        @pl.when(inner == 1)
+        def _():
+            for c in range(CHUNKS):
+                rows_copy(partners[3], c).wait_send()
+                relay_copy(c).wait_send()
+
     for k in range(planes):
         disp_all(k).wait_send()
-    for k in reversed(pairs[0]):
+    for k in (1, 0) if planes > 1 else (0,):
         combine(k, all_tiles)
         back_all(k, all_tiles).wait_send()
-    if len(pairs) > 1:
-        for k in reversed(pairs[1]):
+    if planes > 1:
+        for k in (3, 2):
             for t in range(tiles):
                 combine(k, one_tile[t])
-        for k in pairs[1]:
+        for k in (3, 2):
             back_all(k, all_tiles).wait_send()
     for k in eager:
         for t in range(tiles):
@@ -787,7 +834,6 @@
     experts = n * expert_gate.shape[0]
     capacity = max(2, 2 * seqs * top // experts)
     cap = -(-capacity // 16) * 16
-    slots = n * cap
     planes = 4 if n % 4 == 0 else 1
     plane = n // planes
     qc = w_query.shape[1] // 2
@@ -796,7 +842,8 @@
     positions = key_cache.shape[1]
     hidden = expert_gate.shape[2]
     tiles = half // COL_BLOCK
-    pair_count = 2 if planes == 4 else 1
+    team_count = 3 if planes == 4 else 1
+    most = plane * cap * (2 if planes == 4 else 1)
     keys = jnp.swapaxes(key_cache, 1, 2)
     values = jnp.swapaxes(value_cache, 1, 2)
     operands = (
@@ -819,8 +866,7 @@
     )
     in_smem = (5, 8)
     in_specs = [
-        pl.BlockSpec(memory_space=pltpu.SMEM if i in in_smem else pl.ANY)
-        for i in range(len(operands))
+        pl.BlockSpec(memory_space=pl.ANY) for i in range(len(operands))
     ]
     vmem = pl.BlockSpec(memory_space=pltpu.VMEM)
     loaded = [
@@ -828,7 +874,8 @@
     ]
     dma = pltpu.SemaphoreType.DMA
     scratch = (
-        [loaded[0], loaded[0]]
+        [pltpu.SMEM(operands[i].shape, operands[i].dtype) for i in in_smem]
+        + [loaded[0], loaded[0]]
         + loaded[1:]
         + [
             pltpu.VMEM((seqs + PAD, qc + 2 * kcols + 2 * LANES), F32),
@@ -849,32 +896,33 @@
             pltpu.VMEM((planes, plane, cap, half), BF16),
             pltpu.VMEM((planes, plane, cap, half), BF16),
             pltpu.VMEM((planes, plane, cap, half), BF16),
-            pltpu.VMEM((slots // pair_count, hidden), F32),
-            pltpu.VMEM((slots // pair_count, hidden), F32),
-            pltpu.VMEM((pair_count, slots // pair_count, hidden), BF16),
-            pltpu.VMEM((pair_count, tiles, slots // pair_count, COL_BLOCK), BF16),
-            pltpu.VMEM((pair_count, tiles, slots // pair_count, COL_BLOCK), BF16),
-            pltpu.VMEM((tiles, slots // pair_count, COL_BLOCK), BF16),
+            pltpu.VMEM((most, hidden), F32),
+            pltpu.VMEM((most, hidden), F32),
+            pltpu.VMEM((most, hidden), BF16),
+            pltpu.VMEM((tiles, planes, plane * cap, COL_BLOCK), BF16),
+            pltpu.VMEM((tiles, planes, plane * cap, COL_BLOCK), BF16),
+            pltpu.VMEM((tiles, planes, plane * cap, COL_BLOCK), BF16),
             pltpu.VMEM((planes, plane, tiles, cap, COL_BLOCK), BF16),
             pltpu.VMEM((planes, plane, tiles, cap, COL_BLOCK), BF16),
             pltpu.VMEM((planes, tiles, seqs, COL_BLOCK), BF16),
             pltpu.VMEM((planes, tiles, seqs, COL_BLOCK), BF16),
             pltpu.VMEM((seqs, half), F32),
-            dma((len(loaded),)),
+            dma((len(operands),)),
             dma((2 + CHUNKS,)),
             dma((2 + CHUNKS,)),
             dma((planes,)),
             dma((planes,)),
             dma((planes, CHUNKS)),
             dma((planes, CHUNKS)),
+            dma((CHUNKS,)),
             dma((planes, tiles)),
             dma((planes, tiles)),
             dma((planes,)),
             dma((planes,)),
             dma((planes,)),
             dma((planes,)),
-            dma((pair_count, tiles)),
-            dma((pair_count, tiles)),
+            dma((team_count, tiles)),
+            dma((team_count, tiles)),
             dma((planes,)),
             dma((planes, tiles)),
             dma((planes,)),

time: 43 us -> 40.3 us (0.937)
  Pallas kernels: 42.2 us -> 39.5 us
    pallas_call x1, Pallas kernels: 41.5 us -> 38.8 us  [local(): pl.pallas_call(functools.partial(kernel, n, cap), out_shape=tuple((pltpu....]
where the time goes in v3:
time: 40.3 us; the launch traced here: 40.1 us
  Pallas kernels  39.5 us (98%)
  between operations  0.65 us (2%)
    pallas_call x1, Pallas kernels, local(): pl.pallas_call(functools.partial(kernel, n, cap), out_shape=tuple((pltpu....  38.8 us

profile of v3, /device:TPU:0, one launch (start us, length us, event | category | flops | bytes accessed | tf_op | source)
XLA Modules:
  0.0 40.1 jit_solution(5052392043678127298)
XLA Ops:
  0.6 38.8 %shard_map.175 = (bf16[32,1024]{1,0:T(8,128)(2,1)S(1)}, bf16[32,64]{1,0:T(8,128)(2,1)S(1)}, bf16[32,64]{1,0:T(8,128)(2,1)S(1)}) custom-call(bf16[32,1024]{1,0:T(8,128)(2,1)} %tok_hbm.1, f32[1,1024]{1,0:T(1,128)} %bitcast.14, bf16[1024,1024]{1,0:T(8,128)(2,1)} %wq_hbm.1, bf16[1024,128]{1,0:T(8,128)(2,1)} %wk_hbm.1, bf16[1024,128]{1,0:T(8,128)(2,1)} %wv_hbm.1, ...), custom_call_target="tpu_custom_call" | custom-call | tf_op jit(solution)/shard_map/pallas_call | solution.py:933
  39.5 0.7 %shard_map.176 = (bf16[32,1024]{1,0:T(8,128)(2,1)}, bf16[32,64]{1,0:T(8,128)(2,1)}, bf16[32,64]{1,0:T(8,128)(2,1)}) custom-call(bf16[32,1024]{1,0:T(8,128)(2,1)S(1)} %get-tuple-element.6.refs_0_, bf16[32,64]{1,0:T(8,128)(2,1)S(1)} %get-tuple-element.7.refs_1_, bf16[32,64]{1,0:T(8,128)(2,1)S(1)} %get-tuple-element.8.refs_2_), custom_call_target="tpu_custom_call" | custom-call | tf_op jit(solution)/shard_map/pallas_call | solution.py:943

commit v4 on v3

--- a/solution.py
+++ b/solution.py
@@ -104,7 +104,6 @@
     route_recv_sem,
     rows_send_sem,
     rows_recv_sem,
-    relay_sem,
     sum_send_sem,
     sum_recv_sem,
     disp_send_sem,
@@ -115,8 +114,6 @@
     down_recv_sem,
     back_send_sem,
     back_recv_sem,
-    local_sem,
-    back_local_sem,
 ):
     ep = lax.axis_index("ep")
     tp = lax.axis_index("tp")
@@ -144,16 +141,26 @@
         (lens_hbm, lens_ref),
     )
     for i, (src, dst) in enumerate(pairs):
-        copy = pltpu.make_async_copy(src, dst, load_sem.at[i])
-        loads.append(copy)
+        slot = (10, 11, 12, 11, 12)[i - 11] if i > 10 else i
+        loads.append(pltpu.make_async_copy(src, dst, load_sem.at[slot]))
     for i in (0, 1, 2, 3, 4, 14, 15, 9, 10, 8, 5, 6, 7):
         loads[i].start()
+
+    def tally(ref, sem):
+        return pltpu.make_async_remote_copy(
+            src_ref=ref,
+            dst_ref=ref,
+            send_sem=sem,
+            recv_sem=sem,
+            device_id=(ep, other),
+            device_id_type=MESH,
+        )
 
     def peer_copy(src, dst, i):
         return pltpu.make_async_remote_copy(
             src_ref=src,
             dst_ref=dst,
-            send_sem=one_send.at[i],
+            send_sem=one_send.at[min(i, 1)],
             recv_sem=one_recv.at[i],
             device_id=(ep, other),
             device_id_type=MESH,
@@ -237,19 +244,19 @@
     route_send[:top] = ids[...].astype(F32)
     route_send[top:] = logits[...]
 
-    def route_copy(i, mine):
+    def route_copy(i):
         to = partners[i]
         return pltpu.make_async_remote_copy(
             src_ref=route_send,
-            dst_ref=route_recv.at[level if mine else to],
-            send_sem=route_send_sem.at[to],
-            recv_sem=route_recv_sem.at[level if mine else to],
+            dst_ref=route_recv.at[level],
+            send_sem=route_send_sem.at[0],
+            recv_sem=route_recv_sem.at[0],
             device_id=(to * plane + spot, tp),
             device_id_type=MESH,
         )
 
     for i in eager:
-        route_copy(i, True).start()
+        route_copy(i).start()
     tok_copy = peer_copy(x_own, x_peer, 0)
     tok_copy.start()
 
@@ -392,8 +399,8 @@
         return pltpu.make_async_remote_copy(
             src_ref=rows_ref.at[c],
             dst_ref=rows_recv.at[level, c],
-            send_sem=rows_send_sem.at[to, c],
-            recv_sem=rows_recv_sem.at[level, c],
+            send_sem=rows_send_sem.at[0],
+            recv_sem=rows_recv_sem.at[level],
             device_id=(to * plane + spot, tp),
             device_id_type=MESH,
         )
@@ -403,20 +410,9 @@
         return pltpu.make_async_remote_copy(
             src_ref=rows_recv.at[far, c],
             dst_ref=rows_recv.at[far, c],
-            send_sem=relay_sem.at[c],
-            recv_sem=rows_recv_sem.at[far, c],
+            send_sem=rows_send_sem.at[0],
+            recv_sem=rows_recv_sem.at[far],
             device_id=(partners[2] * plane + spot, tp),
-            device_id_type=MESH,
-        )
-
-    def rows_arrival(i, c):
-        source = partners[i]
-        return pltpu.make_async_remote_copy(
-            src_ref=rows_ref.at[c],
-            dst_ref=rows_recv.at[source, c],
-            send_sem=rows_send_sem.at[source, c],
-            recv_sem=rows_recv_sem.at[source, c],
-            device_id=(source * plane + spot, tp),
             device_id_type=MESH,
         )
 
@@ -460,8 +456,8 @@
         read(c)
         project(c)
     for k in range(planes):
-        if k > 0:
-            route_copy(k, False).wait_recv()
+        if k == 1:
+            tally(route_recv.at[pl.ds(0, planes - 1)], route_recv_sem.at[0]).wait_recv()
         make_tables(k)
     settle(CHUNKS - 1)
 
@@ -480,29 +476,19 @@
         return beside_copy(
             lambda to: disp.at[k, to],
             lambda giver: recv_own.at[k, giver],
-            disp_send_sem.at[k],
+            disp_send_sem.at[0],
             disp_recv_sem.at[k],
             j,
         )
 
-    def disp_all(k):
-        return pltpu.make_async_remote_copy(
-            src_ref=disp.at[k, pl.ds(0, plane - 1)],
-            dst_ref=recv_own.at[k, pl.ds(0, plane - 1)],
-            send_sem=disp_send_sem.at[k],
-            recv_sem=disp_recv_sem.at[k],
-            device_id=(ep, other),
-            device_id_type=MESH,
-        )
-
     def disp_keep(k):
-        return pltpu.make_async_copy(disp.at[k, spot], recv_own.at[k, spot], local_sem.at[k])
+        return pltpu.make_async_copy(disp.at[k, spot], recv_own.at[k, spot], load_sem.at[k])
 
     def fwd_copy(k):
         return pltpu.make_async_remote_copy(
             src_ref=recv_own.at[k],
             dst_ref=recv_peer.at[k],
-            send_sem=fwd_send_sem.at[k],
+            send_sem=fwd_send_sem.at[0],
             recv_sem=fwd_recv_sem.at[k],
             device_id=(ep, other),
             device_id_type=MESH,
@@ -520,12 +506,12 @@
         disp_keep(k).start()
 
     def receive_rows(k):
-        for c in range(CHUNKS):
-            rows_arrival(k, c).wait_recv()
+        source = partners[k]
+        tally(rows_recv.at[source], rows_recv_sem.at[source]).wait_recv()
 
     def gather(k):
         disp_keep(k).wait()
-        disp_all(k).wait_recv()
+        tally(recv_own.at[k, pl.ds(0, plane - 1)], disp_recv_sem.at[k]).wait_recv()
         fwd_copy(k).start()
 
     hidden = gate.shape[1]
@@ -588,11 +574,12 @@
     def down_copy(p, at):
         team = teams[p]
         ks = pl.ds(team[0], len(team))
+        slot = p + at.start // at.size
         return pltpu.make_async_remote_copy(
             src_ref=down_send.at[at, ks],
             dst_ref=down_recv.at[at, ks],
-            send_sem=down_send_sem.at[p, at.start // at.size],
-            recv_sem=down_recv_sem.at[p, at.start // at.size],
+            send_sem=down_send_sem.at[0],
+            recv_sem=down_recv_sem.at[slot],
             device_id=(ep, other),
             device_id_type=MESH,
         )
@@ -616,30 +603,23 @@
                 down_tile(down_send, p, other, t)
             down_copy(p, at).start()
 
+    def back_slot(k, at):
+        return k + at.start // at.size + (tiles - 1 if k == 3 else 0)
+
     def back_copy(k, at, j):
         return beside_copy(
             lambda to: back_send.at[k, to, at],
             lambda giver: back_recv.at[k, giver, at],
-            back_send_sem.at[k],
-            back_recv_sem.at[k, at.start // at.size],
+            back_send_sem.at[0],
+            back_recv_sem.at[back_slot(k, at)],
             j,
-        )
-
-    def back_all(k, at):
-        return pltpu.make_async_remote_copy(
-            src_ref=back_send.at[k, pl.ds(0, plane - 1), at],
-            dst_ref=back_recv.at[k, pl.ds(0, plane - 1), at],
-            send_sem=back_send_sem.at[k],
-            recv_sem=back_recv_sem.at[k, at.start // at.size],
-            device_id=(ep, other),
-            device_id_type=MESH,
         )
 
     def back_keep(k, at):
         return pltpu.make_async_copy(
             back_send.at[k, spot, at],
             back_recv.at[k, spot, at],
-            back_local_sem.at[k, at.start // at.size],
+            load_sem.at[planes + back_slot(k, at)],
         )
 
     def send_back(k, at):
@@ -657,7 +637,7 @@
             down_tile(down_own, p, tp, t)
 
     def join_whole(p):
-        down_copy(p, all_tiles).wait()
+        down_copy(p, all_tiles).wait_recv()
         for t in range(tiles):
             down_join(p, t)
         for k in teams[p]:
@@ -666,7 +646,7 @@
     def join_tiles(p):
         for t in range(tiles):
             down_tile(down_own, p, tp, t)
-            down_copy(p, one_tile[t]).wait()
+            down_copy(p, one_tile[t]).wait_recv()
             down_join(p, t)
             send_back(teams[p][-1], one_tile[t])
         for k in reversed(teams[p][:-1]):
@@ -678,28 +658,18 @@
         return pltpu.make_async_remote_copy(
             src_ref=sum_send.at[to, t],
             dst_ref=sum_recv.at[level, t],
-            send_sem=sum_send_sem.at[to, t],
-            recv_sem=sum_recv_sem.at[level, t],
+            send_sem=sum_send_sem.at[0],
+            recv_sem=sum_recv_sem.at[0],
             device_id=(to * plane + spot, tp),
             device_id_type=MESH,
         )
 
-    def sum_arrival(k, t):
-        source = partners[k]
-        return pltpu.make_async_remote_copy(
-            src_ref=sum_send.at[source, t],
-            dst_ref=sum_recv.at[source, t],
-            send_sem=sum_send_sem.at[source, t],
-            recv_sem=sum_recv_sem.at[source, t],
-            device_id=(source * plane + spot, tp),
-            device_id_type=MESH,
-        )
-
     over_slots = (((0,), (0,)), ((), ()))
 
     def combine(k, at):
         back_keep(k, at).wait()
-        back_all(k, at).wait_recv()
+        arrived = back_recv.at[k, pl.ds(0, plane - 1), at]
+        tally(arrived, back_recv_sem.at[back_slot(k, at)]).wait_recv()
         to = partners[k]
         mixes = []
         for t in range(at.start, at.start + at.size):
@@ -739,7 +709,7 @@
         place_rows(2)
     for i in (11, 12, 13):
         loads[i].wait()
-    fwd_copy(0).wait()
+    fwd_copy(0).wait_recv()
     whole_depth(teams[0])
     down_other(0, [all_tiles])
     if planes > 1:
@@ -750,42 +720,38 @@
     if planes > 1:
         gather(1)
         first_half(teams[1])
-        fwd_copy(1).wait()
+        fwd_copy(1).wait_recv()
         second_half(teams[1])
         down_other(1, [all_tiles])
         gather(2)
         gather(3)
         down_mine(1)
         join_whole(1)
-        fwd_copy(2).wait()
-        fwd_copy(3).wait()
+        fwd_copy(2).wait_recv()
+        fwd_copy(3).wait_recv()
         run_far()
-        for i in range(1, planes):
-            route_copy(i, True).wait_send()
-        for c in range(CHUNKS):
-            rows_copy(partners[1], c).wait_send()
-            rows_copy(partners[2], c).wait_send()
+        tally(route_recv.at[pl.ds(0, planes - 1)], route_send_sem.at[0]).wait_send()
 
         @pl.when(inner == 1)
         def _():
-            for c in range(CHUNKS):
-                rows_copy(partners[3], c).wait_send()
-                relay_copy(c).wait_send()
-
-    for k in range(planes):
-        disp_all(k).wait_send()
+            tally(rows_recv, rows_send_sem.at[0]).wait_send()
+
+        @pl.when(inner == 0)
+        def _():
+            tally(rows_recv.at[pl.ds(0, 2)], rows_send_sem.at[0]).wait_send()
+
+    tally(disp.at[:, pl.ds(0, plane - 1)], disp_send_sem.at[0]).wait_send()
+    tally(recv_own, fwd_send_sem.at[0]).wait_send()
+    tally(down_send, down_send_sem.at[0]).wait_send()
     for k in (1, 0) if planes > 1 else (0,):
         combine(k, all_tiles)
-        back_all(k, all_tiles).wait_send()
     if planes > 1:
         for k in (3, 2):
             for t in range(tiles):
                 combine(k, one_tile[t])
-        for k in (3, 2):
-            back_all(k, all_tiles).wait_send()
-    for k in eager:
-        for t in range(tiles):
-            sum_arrival(k, t).wait_recv()
+    tally(back_send.at[:, pl.ds(0, plane - 1)], back_send_sem.at[0]).wait_send()
+    if planes > 1:
+        tally(sum_recv.at[pl.ds(0, planes - 1)], sum_recv_sem.at[0]).wait_recv()
     for t in range(tiles):
         cols = slice(t * COL_BLOCK, (t + 1) * COL_BLOCK)
         total = total_ref[:, cols]
@@ -793,9 +759,8 @@
             total = total + sum_recv[partners[k], t].astype(F32)
         out_ref[:, cols] = total.astype(BF16)
 
-    for i in range(1, planes):
-        for t in range(tiles):
-            sum_copy(i, t).wait_send()
+    if planes > 1:
+        tally(sum_send.at[pl.ds(0, planes - 1)], sum_send_sem.at[0]).wait_send()
 
 
 def publish(*refs):
@@ -907,26 +872,23 @@
             pltpu.VMEM((planes, tiles, seqs, COL_BLOCK), BF16),
             pltpu.VMEM((planes, tiles, seqs, COL_BLOCK), BF16),
             pltpu.VMEM((seqs, half), F32),
-            dma((len(operands),)),
+            dma((13,)),
+            dma((2,)),
             dma((2 + CHUNKS,)),
-            dma((2 + CHUNKS,)),
+            dma((1,)),
+            dma((1,)),
+            dma((1,)),
             dma((planes,)),
+            dma((1,)),
+            dma((1,)),
+            dma((1,)),
             dma((planes,)),
-            dma((planes, CHUNKS)),
-            dma((planes, CHUNKS)),
-            dma((CHUNKS,)),
-            dma((planes, tiles)),
-            dma((planes, tiles)),
+            dma((1,)),
             dma((planes,)),
-            dma((planes,)),
-            dma((planes,)),
-            dma((planes,)),
-            dma((team_count, tiles)),
-            dma((team_count, tiles)),
-            dma((planes,)),
-            dma((planes, tiles)),
-            dma((planes,)),
-            dma((planes, tiles)),
+            dma((1,)),
+            dma((2 + tiles,)),
+            dma((1,)),
+            dma((2 + 2 * tiles,)),
         ]
     )
     shapes = ((seqs, half), (seqs, kcols), (seqs, kcols))

time: 40.3 us -> 39.5 us (0.980)
  Pallas kernels: 39.5 us -> 38.7 us
    pallas_call x1, Pallas kernels: 38.8 us -> 38 us  [local(): pl.pallas_call(functools.partial(kernel, n, cap), out_shape=tuple((pltpu....]
where the time goes in v4:
time: 39.5 us; the launch traced here: 39.3 us
  Pallas kernels  38.7 us (98%)
  between operations  0.65 us (2%)
    pallas_call x1, Pallas kernels, local(): pl.pallas_call(functools.partial(kernel, n, cap), out_shape=tuple((pltpu....  38 us

profile of v4, /device:TPU:0, one launch (start us, length us, event | category | flops | bytes accessed | tf_op | source)
XLA Modules:
  0.0 39.3 jit_solution(16566164897423089618)
XLA Ops:
  0.6 38.0 %shard_map.175 = (bf16[32,1024]{1,0:T(8,128)(2,1)S(1)}, bf16[32,64]{1,0:T(8,128)(2,1)S(1)}, bf16[32,64]{1,0:T(8,128)(2,1)S(1)}) custom-call(bf16[32,1024]{1,0:T(8,128)(2,1)} %tok_hbm.1, f32[1,1024]{1,0:T(1,128)} %bitcast.14, bf16[1024,1024]{1,0:T(8,128)(2,1)} %wq_hbm.1, bf16[1024,128]{1,0:T(8,128)(2,1)} %wk_hbm.1, bf16[1024,128]{1,0:T(8,128)(2,1)} %wv_hbm.1, ...), custom_call_target="tpu_custom_call" | custom-call | tf_op jit(solution)/shard_map/pallas_call | solution.py:895
  38.7 0.7 %shard_map.176 = (bf16[32,1024]{1,0:T(8,128)(2,1)}, bf16[32,64]{1,0:T(8,128)(2,1)}, bf16[32,64]{1,0:T(8,128)(2,1)}) custom-call(bf16[32,1024]{1,0:T(8,128)(2,1)S(1)} %get-tuple-element.6.refs_0_, bf16[32,64]{1,0:T(8,128)(2,1)S(1)} %get-tuple-element.7.refs_1_, bf16[32,64]{1,0:T(8,128)(2,1)S(1)} %get-tuple-element.8.refs_2_), custom_call_target="tpu_custom_call" | custom-call | tf_op jit(solution)/shard_map/pallas_call | solution.py:905

commit v5 on v4

--- a/solution.py
+++ b/solution.py
@@ -17,7 +17,8 @@
 DEAD = -1e30
 POS_BLOCK = 256
 COL_BLOCK = 512
-GATE_BLOCK = 512
+GATE_BLOCK = 1024
+BACK_BLOCK = 256
 PAD = 16
 BATCH = 4
 CHUNKS = 2
@@ -81,6 +82,7 @@
     route_send,
     route_recv,
     tables,
+    mixing,
     rows_ref,
     rows_recv,
     disp,
@@ -290,10 +292,11 @@
         rank = dot(hot.astype(BF16), earlier)
         chosen = (hot > 0.5) & (jnp.abs(rank - slot_rank) < 0.5)
         weight = jnp.where(chosen, prob_hot, 0.0)
+        tables[k] = jnp.where(chosen, 1.0, 0.0).astype(BF16)
+        weight = weight.T
         weight_hi = weight.astype(BF16)
-        tables[k, 0] = jnp.where(chosen, 1.0, 0.0).astype(BF16)
-        tables[k, 1] = weight_hi
-        tables[k, 2] = (weight - weight_hi.astype(F32)).astype(BF16)
+        mixing[k, :, :group] = weight_hi.astype(F32)
+        mixing[k, :, group:] = weight - weight_hi.astype(F32)
 
     groups = qc // HEAD
     loads[14].wait()
@@ -318,7 +321,7 @@
         )
         return (scale * (own[:seqs] + proj_recv[:seqs, lo:hi] + apart * tilt)).astype(BF16)
 
-    query = joined(own_q, 0, qc).astype(F32)
+    query = joined(own_q, 0, qc).astype(F32) * HEAD ** (-0.5)
     nk_ref[...] = joined(own_k, qc, qc + kcols)
     nv_ref[...] = joined(own_v, qc + kcols, used)
     for h in range(groups):
@@ -351,7 +354,7 @@
             length = jnp.zeros((step_rows, 1), jnp.int32)
             for j in range(BATCH):
                 length = jnp.where(step_seq == j, lens_ref[i * BATCH + j], length)
-            s = dot(q_wide[rows, :], keys) * HEAD ** (-0.5) + step_bias
+            s = dot(q_wide[rows, :], keys) + step_bias
             z_ref[rows, :] = jnp.where(place < length, s, DEAD)
 
     def spend(c):
@@ -499,7 +502,7 @@
             rows = rows_recv[partners[k]].reshape(seqs, half)
         else:
             rows = rows_ref[...].reshape(seqs, half)
-        placed = dot(tables[k, 0], rows).astype(BF16)
+        placed = dot(tables[k], rows).astype(BF16)
         disp[k] = placed.reshape(plane, cap, half)
         for j in range(1, plane):
             disp_copy(k, j).start()
@@ -570,11 +573,15 @@
     tiles = half // COL_BLOCK
     all_tiles = pl.ds(0, tiles)
     one_tile = [pl.ds(t, 1) for t in range(tiles)]
+    backs = half // BACK_BLOCK
+    all_backs = pl.ds(0, backs)
+    one_back = [pl.ds(b, 1) for b in range(backs)]
+    some_backs = [pl.ds(t * backs // tiles, backs // tiles) for t in range(tiles)]
 
     def down_copy(p, at):
         team = teams[p]
         ks = pl.ds(team[0], len(team))
-        slot = p + at.start // at.size
+        slot = p + at.start // at.size + (tiles - 1 if p == 2 else 0)
         return pltpu.make_async_remote_copy(
             src_ref=down_send.at[at, ks],
             dst_ref=down_recv.at[at, ks],
@@ -604,7 +611,8 @@
             down_copy(p, at).start()
 
     def back_slot(k, at):
-        return k + at.start // at.size + (tiles - 1 if k == 3 else 0)
+        base = (0, 1, 1 + tiles, 1 + tiles + backs)[k]
+        return base + at.start // at.size
 
     def back_copy(k, at, j):
         return beside_copy(
@@ -630,7 +638,10 @@
     def down_join(p, t):
         for k in teams[p]:
             total = (down_own[t, k].astype(F32) + down_recv[t, k].astype(F32)).astype(BF16)
-            back_send[k, :, t] = total.reshape(plane, cap, COL_BLOCK)
+            for i in range(COL_BLOCK // BACK_BLOCK):
+                piece = total[:, i * BACK_BLOCK : (i + 1) * BACK_BLOCK]
+                at = t * (COL_BLOCK // BACK_BLOCK) + i
+                back_send[k, :, at] = piece.reshape(plane, cap, BACK_BLOCK)
 
     def down_mine(p):
         for t in range(tiles):
@@ -641,17 +652,18 @@
         for t in range(tiles):
             down_join(p, t)
         for k in teams[p]:
-            send_back(k, all_tiles)
+            send_back(k, all_backs)
 
     def join_tiles(p):
         for t in range(tiles):
             down_tile(down_own, p, tp, t)
             down_copy(p, one_tile[t]).wait_recv()
             down_join(p, t)
-            send_back(teams[p][-1], one_tile[t])
+            for b in range(t * backs // tiles, (t + 1) * backs // tiles):
+                send_back(teams[p][-1], one_back[b])
         for k in reversed(teams[p][:-1]):
-            for t in range(tiles):
-                send_back(k, one_tile[t])
+            for b in range(backs):
+                send_back(k, one_back[b])
 
     def sum_copy(k, t):
         to = partners[k]
@@ -664,8 +676,6 @@
             device_id_type=MESH,
         )
 
-    over_slots = (((0,), (0,)), ((), ()))
-
     def combine(k, at):
         back_keep(k, at).wait()
         arrived = back_recv.at[k, pl.ds(0, plane - 1), at]
@@ -673,13 +683,10 @@
         to = partners[k]
         mixes = []
         for t in range(at.start, at.start + at.size):
-            back = back_recv[k, :, t].reshape(group, COL_BLOCK)
-            mixes.append(
-                lax.dot_general(tables[k, 1], back, over_slots, preferred_element_type=F32)
-                + lax.dot_general(tables[k, 2], back, over_slots, preferred_element_type=F32)
-            )
+            back = back_recv[k, :, t].reshape(group, BACK_BLOCK)
+            mixes.append(dot(mixing[k].astype(BF16), jnp.concatenate([back, back], axis=0)))
         for t, mixed in zip(range(at.start, at.start + at.size), mixes):
-            cols = slice(t * COL_BLOCK, (t + 1) * COL_BLOCK)
+            cols = slice(t * BACK_BLOCK, (t + 1) * BACK_BLOCK)
             if k == 0:
                 total_ref[:, cols] = res_ref[:, cols].astype(F32) + mixed
             else:
@@ -709,8 +716,9 @@
         place_rows(2)
     for i in (11, 12, 13):
         loads[i].wait()
+    first_half(teams[0])
     fwd_copy(0).wait_recv()
-    whole_depth(teams[0])
+    second_half(teams[0])
     down_other(0, [all_tiles])
     if planes > 1:
         receive_rows(3)
@@ -722,11 +730,14 @@
         first_half(teams[1])
         fwd_copy(1).wait_recv()
         second_half(teams[1])
-        down_other(1, [all_tiles])
+        down_other(1, one_tile)
         gather(2)
         gather(3)
         down_mine(1)
-        join_whole(1)
+        for t in range(tiles):
+            down_copy(1, one_tile[t]).wait_recv()
+            down_join(1, t)
+            send_back(1, some_backs[t])
         fwd_copy(2).wait_recv()
         fwd_copy(3).wait_recv()
         run_far()
@@ -743,17 +754,19 @@
     tally(disp.at[:, pl.ds(0, plane - 1)], disp_send_sem.at[0]).wait_send()
     tally(recv_own, fwd_send_sem.at[0]).wait_send()
     tally(down_send, down_send_sem.at[0]).wait_send()
-    for k in (1, 0) if planes > 1 else (0,):
-        combine(k, all_tiles)
+    if planes > 1:
+        for at in some_backs:
+            combine(1, at)
+    combine(0, all_backs)
     if planes > 1:
         for k in (3, 2):
-            for t in range(tiles):
-                combine(k, one_tile[t])
+            for b in range(backs):
+                combine(k, one_back[b])
     tally(back_send.at[:, pl.ds(0, plane - 1)], back_send_sem.at[0]).wait_send()
     if planes > 1:
         tally(sum_recv.at[pl.ds(0, planes - 1)], sum_recv_sem.at[0]).wait_recv()
-    for t in range(tiles):
-        cols = slice(t * COL_BLOCK, (t + 1) * COL_BLOCK)
+    for t in range(backs):
+        cols = slice(t * BACK_BLOCK, (t + 1) * BACK_BLOCK)
         total = total_ref[:, cols]
         for k in range(1, planes):
             total = total + sum_recv[partners[k], t].astype(F32)
@@ -807,7 +820,7 @@
     positions = key_cache.shape[1]
     hidden = expert_gate.shape[2]
     tiles = half // COL_BLOCK
-    team_count = 3 if planes == 4 else 1
+    backs = half // BACK_BLOCK
     most = plane * cap * (2 if planes == 4 else 1)
     keys = jnp.swapaxes(key_cache, 1, 2)
     values = jnp.swapaxes(value_cache, 1, 2)
@@ -855,7 +868,8 @@
             pltpu.VMEM((seqs, half), BF16),
             pltpu.VMEM((2 * top, seqs), F32),
             pltpu.VMEM((planes, 2 * top, seqs), F32),
-            pltpu.VMEM((planes, 3, plane * cap, seqs), BF16),
+            pltpu.VMEM((planes, plane * cap, seqs), BF16),
+            pltpu.VMEM((planes, seqs, 2 * plane * cap), F32),
             pltpu.VMEM((CHUNKS, seqs // CHUNKS, half), BF16),
             pltpu.VMEM((planes, CHUNKS, seqs // CHUNKS, half), BF16),
             pltpu.VMEM((planes, plane, cap, half), BF16),
@@ -867,12 +881,12 @@
             pltpu.VMEM((tiles, planes, plane * cap, COL_BLOCK), BF16),
             pltpu.VMEM((tiles, planes, plane * cap, COL_BLOCK), BF16),
             pltpu.VMEM((tiles, planes, plane * cap, COL_BLOCK), BF16),
-            pltpu.VMEM((planes, plane, tiles, cap, COL_BLOCK), BF16),
-            pltpu.VMEM((planes, plane, tiles, cap, COL_BLOCK), BF16),
-            pltpu.VMEM((planes, tiles, seqs, COL_BLOCK), BF16),
-            pltpu.VMEM((planes, tiles, seqs, COL_BLOCK), BF16),
+            pltpu.VMEM((planes, plane, backs, cap, BACK_BLOCK), BF16),
+            pltpu.VMEM((planes, plane, backs, cap, BACK_BLOCK), BF16),
+            pltpu.VMEM((planes, backs, seqs, BACK_BLOCK), BF16),
+            pltpu.VMEM((planes, backs, seqs, BACK_BLOCK), BF16),
             pltpu.VMEM((seqs, half), F32),
-            dma((13,)),
+            dma((planes + 1 + tiles + 2 * backs,)),
             dma((2,)),
             dma((2 + CHUNKS,)),
             dma((1,)),
@@ -886,9 +900,9 @@
             dma((1,)),
             dma((planes,)),
             dma((1,)),
-            dma((2 + tiles,)),
+            dma((1 + 2 * tiles,)),
             dma((1,)),
-            dma((2 + 2 * tiles,)),
+            dma((1 + tiles + 2 * backs,)),
         ]
     )
     shapes = ((seqs, half), (seqs, kcols), (seqs, kcols))

time: 39.5 us -> 38.1 us (0.965)
  Pallas kernels: 38.7 us -> 37.3 us
    pallas_call x1, Pallas kernels: 38 us -> 36.6 us  [local(): pl.pallas_call(functools.partial(kernel, n, cap), out_shape=tuple((pltpu....]
where the time goes in v5:
time: 38.1 us; the launch traced here: 37.9 us
  Pallas kernels  37.3 us (98%)
  between operations  0.65 us (2%)
    pallas_call x1, Pallas kernels, local(): pl.pallas_call(functools.partial(kernel, n, cap), out_shape=tuple((pltpu....  36.6 us

profile of v5, /device:TPU:0, one launch (start us, length us, event | category | flops | bytes accessed | tf_op | source)
XLA Modules:
  0.0 37.9 jit_solution(15427830797651581362)
XLA Ops:
  0.6 36.6 %shard_map.175 = (bf16[32,1024]{1,0:T(8,128)(2,1)S(1)}, bf16[32,64]{1,0:T(8,128)(2,1)S(1)}, bf16[32,64]{1,0:T(8,128)(2,1)S(1)}) custom-call(bf16[32,1024]{1,0:T(8,128)(2,1)} %tok_hbm.1, f32[1,1024]{1,0:T(1,128)} %bitcast.14, bf16[1024,1024]{1,0:T(8,128)(2,1)} %wq_hbm.1, bf16[1024,128]{1,0:T(8,128)(2,1)} %wk_hbm.1, bf16[1024,128]{1,0:T(8,128)(2,1)} %wv_hbm.1, ...), custom_call_target="tpu_custom_call" | custom-call | tf_op jit(solution)/shard_map/pallas_call | solution.py:909
  37.3 0.7 %shard_map.176 = (bf16[32,1024]{1,0:T(8,128)(2,1)}, bf16[32,64]{1,0:T(8,128)(2,1)}, bf16[32,64]{1,0:T(8,128)(2,1)}) custom-call(bf16[32,1024]{1,0:T(8,128)(2,1)S(1)} %get-tuple-element.6.refs_0_, bf16[32,64]{1,0:T(8,128)(2,1)S(1)} %get-tuple-element.7.refs_1_, bf16[32,64]{1,0:T(8,128)(2,1)S(1)} %get-tuple-element.8.refs_2_), custom_call_target="tpu_custom_call" | custom-call | tf_op jit(solution)/shard_map/pallas_call | solution.py:919

commit v6 on v5

--- a/solution.py
+++ b/solution.py
@@ -730,8 +730,8 @@
         first_half(teams[1])
         fwd_copy(1).wait_recv()
         second_half(teams[1])
+        gather(2)
         down_other(1, one_tile)
-        gather(2)
         gather(3)
         down_mine(1)
         for t in range(tiles):

time: 38.1 us -> 38.1 us (level)
  no operation moved by 1% of the time
where the time goes in v6:
time: 38.1 us; the launch traced here: 37.9 us
  Pallas kernels  37.3 us (98%)
  between operations  0.65 us (2%)
    pallas_call x1, Pallas kernels, local(): pl.pallas_call(functools.partial(kernel, n, cap), out_shape=tuple((pltpu....  36.6 us

profile of v6, /device:TPU:0, one launch (start us, length us, event | category | flops | bytes accessed | tf_op | source)
XLA Modules:
  0.0 37.9 jit_solution(4157677961305342250)
XLA Ops:
  0.6 36.6 %shard_map.175 = (bf16[32,1024]{1,0:T(8,128)(2,1)S(1)}, bf16[32,64]{1,0:T(8,128)(2,1)S(1)}, bf16[32,64]{1,0:T(8,128)(2,1)S(1)}) custom-call(bf16[32,1024]{1,0:T(8,128)(2,1)} %tok_hbm.1, f32[1,1024]{1,0:T(1,128)} %bitcast.14, bf16[1024,1024]{1,0:T(8,128)(2,1)} %wq_hbm.1, bf16[1024,128]{1,0:T(8,128)(2,1)} %wk_hbm.1, bf16[1024,128]{1,0:T(8,128)(2,1)} %wv_hbm.1, ...), custom_call_target="tpu_custom_call" | custom-call | tf_op jit(solution)/shard_map/pallas_call | solution.py:909
  37.2 0.7 %shard_map.176 = (bf16[32,1024]{1,0:T(8,128)(2,1)}, bf16[32,64]{1,0:T(8,128)(2,1)}, bf16[32,64]{1,0:T(8,128)(2,1)}) custom-call(bf16[32,1024]{1,0:T(8,128)(2,1)S(1)} %get-tuple-element.6.refs_0_, bf16[32,64]{1,0:T(8,128)(2,1)S(1)} %get-tuple-element.7.refs_1_, bf16[32,64]{1,0:T(8,128)(2,1)S(1)} %get-tuple-element.8.refs_2_), custom_call_target="tpu_custom_call" | custom-call | tf_op jit(solution)/shard_map/pallas_call | solution.py:919
